TPU v7x, 32 devices: a whole 2x2x4 slice. The times are simulated.
32 devices in a mesh: fs: 16 (over z, y, x), tp: 2 (over core).
Axes of the slice: x: 2, y: 2, z: 4, core: 2. Of those that a mesh axis runs over, the one named last changes fastest.
Arguments:
- gate_pre: bfloat16 [8192, 3072], P('fs', 'tp'), may hold values from -6 to 6
- up_pre: bfloat16 [8192, 3072], P('fs', 'tp'), may hold values from -6 to 6
- cotangent: bfloat16 [8192, 2048], P('fs'), may hold values from -8 to 8
- gate_weight: bfloat16 [2048, 3072], P('fs', 'tp'), may hold values from -0.125 to 0.125
- up_weight: bfloat16 [2048, 3072], P('fs', 'tp'), may hold values from -0.125 to 0.125
- down_weight: bfloat16 [2048, 3072], P('fs', 'tp'), may hold values from -0.109375 to 0.109375
Outputs:
- grad_input: bfloat16 [8192, 2048], P('fs')
- grad_down: float32 [2048, 3072], P('fs', 'tp')
All inputs are finite; a program needn't handle non-finite values.
Results may differ from a plain program's by a relative error of at most 0.014.
Values may be sent and summed in bfloat16 or wider, within the bound.
No kernel may reach another device: no remote copies, remote signals or barrier semaphores. Data moves between devices by JAX's collectives and lax.ppermute only.
A program may use at most 128 MiB of HBM per device.

v0:
```python
import functools
import math

import jax
import jax.numpy as jnp
from jax import lax
from jax.experimental import pallas as pl
from jax.experimental.pallas import tpu as pltpu
from jax.sharding import PartitionSpec as P

F32, BF16 = jnp.float32, jnp.bfloat16
B = 4


def pack_weights_kernel(fb, at_ref, d_ref, g_ref, u_ref, own_ref, *outs):
    for k in range(B):
        at = pl.ds(pl.multiple_of((at_ref[0] ^ k) * fb, 128), fb)
        d, gu = (outs[k - 1], outs[B + k - 2]) if k else (own_ref, own_ref)
        first = 0 if k else fb
        d[:, :fb] = d_ref[:, at]
        gu[:, first : first + fb] = g_ref[:, at]
        gu[:, first + fb : first + 2 * fb] = u_ref[:, at]


def pack_tokens_kernel(fb, rows, tp, at_ref, g_ref, u_ref, *outs):
    for k in range(B):
        at = pl.ds(pl.multiple_of((at_ref[0] ^ k) * fb, 128), fb)
        for h in range(tp):
            here = pl.ds(pl.multiple_of((at_ref[1] ^ h) * rows, 16), rows)
            outs[k][h * rows : (h + 1) * rows, :fb] = g_ref[here, at]
            outs[k][h * rows : (h + 1) * rows, fb:] = u_ref[here, at]


def rows_kernel(wrows, lo, hi, spots, at_ref, *refs):
    *pieces, out_ref = refs
    for j, spot in enumerate(spots):
        own, rest = pieces[2 * j], pieces[2 * j + 1]
        base = spot * B if isinstance(spot, int) else at_ref[2 + spot[0]] * B
        for k in range(B):
            row = pl.multiple_of((base + (at_ref[0] ^ k)) * wrows, 16)
            v = rest[(k - 1) * wrows : k * wrows, :] if k else own[:, lo:hi]
            out_ref[pl.ds(row, wrows), :] = v


def stack_kernel(at_ref, *refs):
    *pieces, out_ref = refs
    row = 0
    for v in pieces:
        out_ref[row : row + v.shape[0], :] = v[...]
        row += v.shape[0]


def result_kernel(rows, at_ref, *refs):
    *pieces, out_ref = refs
    for v, (h, t, lo, width) in zip(pieces, rows[1]):
        here = pl.ds(pl.multiple_of((at_ref[1] ^ h) * rows[0], 16), rows[0])
        for j in range(v.shape[1] // width):
            there = pl.ds(pl.multiple_of(at_ref[2 + t + j] * width, 128), width)
            out_ref[here, there] = v[:, j * width : (j + 1) * width]


def packed(kernel, at, arrays, shapes):
    whole = pl.BlockSpec()
    moved = 2 * sum(v.size for v in arrays) + 2 * sum(math.prod(x) for x in shapes)
    return pl.pallas_call(
        kernel,
        in_specs=[pl.BlockSpec(memory_space=pltpu.SMEM)] + [whole] * len(arrays),
        out_specs=[whole] * len(shapes),
        out_shape=[jax.ShapeDtypeStruct(s, BF16) for s in shapes],
        compiler_params=pltpu.CompilerParams(vmem_limit_bytes=moved + (2 << 20)),
        cost_estimate=pl.CostEstimate(flops=moved, bytes_accessed=moved, transcendentals=0),
    )(at, *arrays)


def make_local(n, tp):
    a = n // B
    order = [0] + list(range(1, a, 2)) + [j for j in range(a - 1, 0, -1) if j % 2 == 0]
    after = {order[j]: order[(j + 1) % a] for j in range(a)}
    last_odd = max([1] + list(range(1, a, 2)))

    def xperm(v, k):
        return lax.ppermute(v, "fs", [(j, (j // B) * B + ((j % B) ^ k)) for j in range(n)])

    def zring(v):
        return lax.ppermute(v, "fs", [(j, after[j // B] * B + j % B) for j in range(n)])

    def zshift(v, s):
        return lax.ppermute(v, "fs", [(j, ((j // B + s) % a) * B + j % B) for j in range(n)])

    def tperm(v, h):
        return lax.ppermute(v, "tp", [(j, j ^ h) for j in range(tp)])

    def source(z):
        odd = jnp.where(z == 1, 0, z - 2)
        even = jnp.where(z + 2 >= a, last_odd, z + 2)
        return jnp.where(z == 0, order[-1], jnp.where(z % 2 == 1, odd, even))

    def put(buf, v, row):
        return lax.dynamic_update_slice_in_dim(buf, v, row, 0)

    def local(g, u, cot, wg, wu, wd):
        i = lax.axis_index("fs")
        c = lax.axis_index("tp")
        q, z = i % B, i // B
        tokens, width = cot.shape
        fb = g.shape[1] // B
        half = tokens // tp
        wrows = wd.shape[0]
        zrows = width // a
        sources = [z]
        for _ in range(1, a):
            sources.append(source(sources[-1]))
        at = jnp.stack([q, c] + sources).astype(jnp.int32)

        def cols(v, j):
            return lax.dynamic_slice_in_dim(v, j * fb, fb, 1)

        def part(v, h):
            return lax.dynamic_slice_in_dim(v, (c ^ h) * half, half, 0)

        tiled = fb % 128 == 0 and wrows % 16 == 0 and zrows % 128 == 0 and half % 32 == 0

        def stacked(got):
            if not tiled:
                return jnp.concatenate(got, 0)
            return packed(stack_kernel, at, got, [(sum(v.shape[0] for v in got), got[0].shape[1])])[0]

        if tiled:
            packs = packed(
                functools.partial(pack_weights_kernel, fb),
                at,
                (wd, wg, wu),
                [(wrows, 3 * fb)] + [(wrows, fb)] * (B - 1) + [(wrows, 2 * fb)] * (B - 1),
            )
            tok = packed(
                functools.partial(pack_tokens_kernel, fb, half, tp),
                at,
                (g, u),
                [(tokens, 2 * fb)] * B,
            )
        else:
            packs = [jnp.concatenate([cols(wd, q), cols(wg, q), cols(wu, q)], 1)]
            packs += [cols(wd, q ^ k) for k in range(1, B)]
            packs += [jnp.concatenate([cols(wg, q ^ k), cols(wu, q ^ k)], 1) for k in range(1, B)]
            tok = [
                jnp.concatenate(
                    [jnp.concatenate([cols(part(v, h), q ^ k) for h in range(tp)], 0) for v in (g, u)], 1
                )
                for k in range(B)
            ]

        ros = [packs[0]]
        rds = [stacked([xperm(packs[k], k) for k in range(1, B)])]
        rgs = [stacked([xperm(packs[B - 1 + k], k) for k in range(1, B)])]
        for _ in range(1, a):
            ros.append(zring(ros[-1]))
            rds.append(zring(rds[-1]))
            rgs.append(zring(rgs[-1]))

        def assembled(ts, rests, lo, hi, natural):
            spots = tuple((t,) if natural else j for j, t in enumerate(ts))
            shape = (len(ts) * B * wrows, hi - lo)
            if tiled:
                pieces = [v for t in ts for v in (ros[t], rests[t])]
                kernel = functools.partial(rows_kernel, wrows, lo, hi, spots)
                return packed(kernel, at, pieces, [shape])[0]
            rows = jnp.zeros(shape, BF16)
            for spot, t in zip(spots, ts):
                base = sources[t] if natural else spot
                for k in range(B):
                    v = rests[t][(k - 1) * wrows : k * wrows] if k else ros[t][:, lo:hi]
                    rows = put(rows, v, (base * B + (q ^ k)) * wrows)
            return rows

        wd_full = assembled(range(a), rds, 0, fb, True)

        mine = part(cot, 0)
        m1 = xperm(mine, 1)
        m2 = xperm(mine, 2)
        cut = half // 2
        m3 = [xperm(m1[:cut], 2), xperm(m2[cut:], 1)]
        own = lax.optimization_barrier((cot, mine))[0]
        cots = [jnp.concatenate([mine] + [part(own, h) for h in range(1, tp)], 0)]
        for got in ([m1], [m2], m3):
            swapped = [tperm(v, h) for h in range(1, tp) for v in got]
            cots.append(stacked(got + swapped))
        gus = [tok[0]] + [xperm(tok[k], k) for k in range(1, B)]

        down = None
        dgus = []
        for k in range(B):
            gate = gus[k][:, :fb].astype(F32)
            upper = gus[k][:, fb:].astype(F32)
            sigma = jax.nn.sigmoid(gate)
            hidden = (gate * sigma * upper).astype(BF16)
            dh = jnp.dot(cots[k], wd_full, preferred_element_type=F32)
            d_gate = (dh * upper * sigma * (1.0 + gate * (1.0 - sigma))).astype(BF16)
            d_up = (dh * gate * sigma).astype(BF16)
            dgus.append(jnp.concatenate([d_gate, d_up], 1))
            term = lax.dot_general(
                cots[k], hidden, (((0,), (0,)), ((), ())), preferred_element_type=F32
            )
            down = term if down is None else down + term

        acc = lax.dynamic_slice_in_dim(down, z * zrows, zrows, 0)
        for s in range(1, a):
            sent = lax.dynamic_slice_in_dim(down, ((z + s) % a) * zrows, zrows, 0).astype(BF16)
            acc = acc + zshift(sent, s).astype(F32)
        got = []
        for k in range(B):
            v = lax.dynamic_slice_in_dim(acc, (q ^ k) * wrows, wrows, 0)
            got.append(xperm(v.astype(BF16), k).astype(F32) if k else v)
        grad_down = jnp.concatenate([lax.select_n(q ^ r, *got) for r in range(B)], 1)

        chunks = [(0, a - 1), (a - 1, a)] if a > 1 else [(0, 1)]
        finished = []
        for t0, t1 in chunks:
            wgu = assembled(range(t0, t1), rgs, fb, 3 * fb, False)
            sums = [None] * B
            for k in (1, 2, 3, 0):
                gi = lax.dot_general(dgus[k], wgu, (((1,), (1,)), ((), ())), preferred_element_type=F32).astype(BF16)
                s = gi[:half].astype(F32)
                for h in range(1, tp):
                    s = s + tperm(gi[h * half : (h + 1) * half], h).astype(F32)
                sums[k] = s
            mid = sums[0].shape[1] // 2
            outs = []
            for first, second, lo, hi in ((1, 2, 0, mid), (2, 1, mid, 2 * mid)):
                direct = xperm(sums[first][:, lo:hi].astype(BF16), first).astype(F32)
                onward = xperm(sums[3][:, lo:hi].astype(BF16), first).astype(F32)
                relay = (sums[second][:, lo:hi] + onward).astype(BF16)
                outs.append((sums[0][:, lo:hi] + direct, xperm(relay, second)))
            finished.append(outs)
        flat = lax.optimization_barrier(([r for outs in finished for _, r in outs], got))[0]
        pieces, places = [], []
        for (t0, t1), outs, late in zip(chunks, finished, [flat[j : j + 2] for j in range(0, len(flat), 2)]):
            own = jnp.concatenate([s + r.astype(F32) for (s, _), r in zip(outs, late)], 1).astype(BF16)
            pieces.append(own)
            places.append((0, t0, 0, zrows))
            for h in range(1, tp):
                pieces.append(tperm(own, h))
                places.append((h, t0, 0, zrows))
        if tiled:
            grad_input = packed(
                functools.partial(result_kernel, (half, tuple(places))), at, pieces, [(tokens, width)]
            )[0]
        else:
            grad_input = jnp.zeros((tokens, width), BF16)
            for v, (h, t, _, wide) in zip(pieces, places):
                for j in range(v.shape[1] // wide):
                    block = v[:, j * wide : (j + 1) * wide]
                    spot = ((c ^ h) * half, sources[t + j] * wide)
                    grad_input = lax.dynamic_update_slice(grad_input, block, spot)
        return grad_input, grad_down

    return local


def solution(mesh):
    n, tp = mesh.shape["fs"], mesh.shape["tp"]
    placed = (
        P("fs", "tp"),
        P("fs", "tp"),
        P("fs", None),
        P("fs", "tp"),
        P("fs", "tp"),
        P("fs", "tp"),
    )
    body = make_local(n, tp)

    return jax.shard_map(
        body,
        mesh=mesh,
        in_specs=placed,
        out_specs=(P("fs", None), P("fs", "tp")),
        check_vma=False,
    )
```

profile of v0, /device:TPU:0, one launch (start us, length us, event | category | flops | bytes accessed | tf_op | source)
XLA Modules:
  0.0 227.8 jit_solution(5135664507727326789)
XLA Ops:
  6.0 3.0 %collective-permute-start.10 = (bf16[128,768]{1,0:T(8,128)(2,1)S(1)}, bf16[128,768]{1,0:T(8,128)(2,1)S(1)}, u32[]{:S(2)}, u32[]{:S(2)}) collective-permute-start(bf16[128,768]{1,0:T(8,128)(2,1)S(1)} %get-tuple-element.25), channel_id=1, source_target_pairs={{0,4},{2,6},{4,0},{6,2},{8,12},{10,14},{12,8},{14,10},{16,20},{18,... | collective-permute-start | bytes 589832 | tf_op jit(solution)/shard_map/ppermute | solution.py:82
  10.5 2.0 collective-permute-start
  12.5 1.5 collective-permute-start.1
  14.0 5.0 %collective-permute-done.10.refs_1_ = bf16[128,768]{1,0:T(8,128)(2,1)S(1)} collective-permute-done((bf16[128,768]{1,0:T(8,128)(2,1)S(1)}, bf16[128,768]{1,0:T(8,128)(2,1)S(1)}, u32[]{:S(2)}, u32[]{:S(2)}) %collective-permute-start.10) | collective-permute-done | bytes 196640 | tf_op jit(solution)/shard_map/ppermute | solution.py:82
  19.0 2.9 %collective-permute-start.2 = (bf16[128,384]{1,0:T(8,128)(2,1)}, bf16[128,384]{1,0:T(8,128)(2,1)S(1)}, u32[]{:S(2)}, u32[]{:S(2)}) collective-permute-start(bf16[128,384]{1,0:T(8,128)(2,1)} %copy-done.9), channel_id=1, source_target_pairs={{0,6},{2,4},{4,2},{6,0},{8,14},{10,12},{12,10},{14,8},{16,22},{18,... | collective-permute-start | bytes 294920 | tf_op jit(solution)/shard_map/ppermute | solution.py:82
  23.2 1.6 collective-permute-start.12
  26.4 2.6 %collective-permute-start.3 = (bf16[128,1152]{1,0:T(8,128)(2,1)}, bf16[128,1152]{1,0:T(8,128)(2,1)}, u32[]{:S(2)}, u32[]{:S(2)}) collective-permute-start(bf16[128,1152]{1,0:T(8,128)(2,1)} %get-tuple-element.19.refs_0_), channel_id=1, source_target_pairs={{0,8},{2,10},{4,12},{6,14},{8,24},{10,26},{12,28},{14,30},{16,0},{... | collective-permute-start | bytes 884744 | tf_op jit(solution)/shard_map/ppermute | solution.py:85
  31.6 15.3 %collective-permute-done.3.refs_2_ = bf16[128,1152]{1,0:T(8,128)(2,1)} collective-permute-done((bf16[128,1152]{1,0:T(8,128)(2,1)}, bf16[128,1152]{1,0:T(8,128)(2,1)}, u32[]{:S(2)}, u32[]{:S(2)}) %collective-permute-start.3) | collective-permute-done | bytes 294944 | tf_op jit(solution)/shard_map/ppermute | solution.py:85
  47.7 5.5 %collective-permute-done.4.refs_3_ = bf16[384,384]{1,0:T(8,128)(2,1)} collective-permute-done((bf16[384,384]{1,0:T(8,128)(2,1)S(1)}, bf16[384,384]{1,0:T(8,128)(2,1)}, u32[]{:S(2)}, u32[]{:S(2)}) %collective-permute-start.4) | collective-permute-done | bytes 294944 | tf_op jit(solution)/shard_map/ppermute | solution.py:85
  58.2 3.5 %collective-permute-start.13 = (bf16[384,768]{1,0:T(8,128)(2,1)}, bf16[384,768]{1,0:T(8,128)(2,1)S(1)}, u32[]{:S(2)}, u32[]{:S(2)}) collective-permute-start(bf16[384,768]{1,0:T(8,128)(2,1)} %collective-permute-done.12.refs_3_), channel_id=1, source_target_pairs={{0,8},{2,10},{4,12},{6,14},{8,24},{10,26},{12,28},{14,30},{16,0},{... | collective-permute-start | bytes 1769480 | tf_op jit(solution)/shard_map/ppermute | solution.py:85
  61.9 4.0 %collective-permute-done.6.refs_5_ = bf16[384,384]{1,0:T(8,128)(2,1)} collective-permute-done((bf16[384,384]{1,0:T(8,128)(2,1)}, bf16[384,384]{1,0:T(8,128)(2,1)}, u32[]{:S(2)}, u32[]{:S(2)}) %collective-permute-start.6) | collective-permute-done | bytes 294944 | tf_op jit(solution)/shard_map/ppermute | solution.py:85
  66.7 2.3 %fusion = f32[2048,384]{0,1:T(8,128)S(1)} fusion(bf16[256,2048]{1,0:T(8,128)(2,1)S(1)} %constant_dynamic-slice_fusion.1, bf16[256,2048]{1,0:T(8,128)(2,1)} %constant_dynamic-slice_fusion.2, bf16[512,768]{1,0:T(8,128)(2,1)S(1)} %get-tuple-element.23), kind=kOutput, calls=%fused_computation.26 | convolution fusion | flops 811073536 | bytes 6029312 | tf_op jit(solution)/shard_map/dot_general | solution.py:200
  69.1 15.6 %collective-permute-done.7.refs_6_.refs_0_ = bf16[128,1152]{1,0:T(8,128)(2,1)S(1)} collective-permute-done((bf16[128,1152]{1,0:T(8,128)(2,1)}, bf16[128,1152]{1,0:T(8,128)(2,1)S(1)}, u32[]{:S(2)}, u32[]{:S(2)}) %collective-permute-start.7) | collective-permute-done | bytes 294944 | tf_op jit(solution)/shard_map/ppermute | solution.py:85
  85.3 2.5 %collective-permute-done.8.refs_7_ = bf16[384,384]{1,0:T(8,128)(2,1)S(1)} collective-permute-done((bf16[384,384]{1,0:T(8,128)(2,1)}, bf16[384,384]{1,0:T(8,128)(2,1)S(1)}, u32[]{:S(2)}, u32[]{:S(2)}) %collective-permute-start.8) | collective-permute-done | bytes 294944 | tf_op jit(solution)/shard_map/ppermute | solution.py:85
  90.5 2.7 %fusion.4 = (bf16[512,384]{1,0:T(8,128)(2,1)S(1)}, bf16[512,384]{1,0:T(8,128)(2,1)S(1)}) fusion(bf16[512,768]{1,0:T(8,128)(2,1)S(1)} %get-tuple-element.23, bf16[2048,384]{1,0:T(8,128)(2,1)S(1)} %shard_map.79, bf16[256,2048]{1,0:T(8,128)(2,1)S(1)} %constant_dynamic-slice_fusion.1, bf16[256,2048]{1,0:T(8,128)(2,1)} %constant_dynamic-slice_fusion.2), kind=kOutput, calls=%fused_computation.42 | convolution fusion | flops 812449792 | bytes 5242880 | tf_op jit(solution)/shard_map/dot_general | solution.py:196
  94.7 1.6 collective-permute-start.25
  96.2 1.7 shard_map.82
  99.4 6.6 %collective-permute-done.34.refs_1_ = bf16[384,768]{1,0:T(8,128)(2,1)S(1)} collective-permute-done((bf16[384,768]{1,0:T(8,128)(2,1)S(1)}, bf16[384,768]{1,0:T(8,128)(2,1)S(1)}, u32[]{:S(2)}, u32[]{:S(2)}) %collective-permute-start.34) | collective-permute-done | bytes 589856 | tf_op jit(solution)/shard_map/ppermute | solution.py:85
  107.6 1.8 collective-permute-start.28
  118.1 23.6 %collective-permute-done.22 = bf16[512,768]{1,0:T(8,128)(2,1)S(1)} collective-permute-done((bf16[512,768]{1,0:T(8,128)(2,1)S(1)}, bf16[512,768]{1,0:T(8,128)(2,1)S(1)}, u32[]{:S(2)}, u32[]{:S(2)}) %collective-permute-start.22) | collective-permute-done | bytes 786464 | tf_op jit(solution)/shard_map/ppermute | solution.py:82
  144.4 2.4 %collective-permute-start.42 = (bf16[512,384]{0,1:T(8,128)(2,1)S(1)}, bf16[512,384]{0,1:T(8,128)(2,1)S(1)}, u32[]{:S(2)}, u32[]{:S(2)}) collective-permute-start(bf16[512,384]{0,1:T(8,128)(2,1)S(1)} %get-tuple-element.38), channel_id=1, source_target_pairs={{0,8},{2,10},{4,12},{6,14},{8,16},{10,18},{12,20},{14,22},{16,24},... | collective-permute-start | bytes 1179656 | tf_op jit(solution)/shard_map/ppermute | solution.py:88
  146.8 1.8 collective-permute-start.43
  160.4 12.5 %collective-permute-done.43 = bf16[512,384]{0,1:T(8,128)(2,1)S(1)} collective-permute-done((bf16[512,384]{0,1:T(8,128)(2,1)S(1)}, bf16[512,384]{0,1:T(8,128)(2,1)S(1)}, u32[]{:S(2)}, u32[]{:S(2)}) %collective-permute-start.43) | collective-permute-done | bytes 393248 | tf_op jit(solution)/shard_map/ppermute | solution.py:88
  173.2 1.5 collective-permute-start.37
  174.9 3.2 %collective-permute-done.40 = bf16[256,256]{1,0:T(8,128)(2,1)S(1)} collective-permute-done((bf16[256,256]{1,0:T(8,128)(2,1)S(1)}, bf16[256,256]{1,0:T(8,128)(2,1)S(1)}, u32[]{:S(2)}, u32[]{:S(2)}) %collective-permute-start.40) | collective-permute-done | bytes 131104 | tf_op jit(solution)/shard_map/ppermute | solution.py:82
  181.4 1.5 collective-permute-start.30
  183.3 7.7 %collective-permute-done.32 = bf16[256,768]{1,0:T(8,128)(2,1)S(1)} collective-permute-done((bf16[256,768]{1,0:T(8,128)(2,1)S(1)}, bf16[256,768]{1,0:T(8,128)(2,1)S(1)}, u32[]{:S(2)}, u32[]{:S(2)}) %collective-permute-start.32) | collective-permute-done | bytes 393248 | tf_op jit(solution)/shard_map/ppermute | solution.py:82
  191.0 1.7 collective-permute-start.47
  201.0 15.2 %collective-permute-done.38 = bf16[256,256]{1,0:T(8,128)(2,1)S(1)} collective-permute-done((bf16[256,256]{1,0:T(8,128)(2,1)S(1)}, bf16[256,256]{1,0:T(8,128)(2,1)S(1)}, u32[]{:S(2)}, u32[]{:S(2)}) %collective-permute-start.38) | collective-permute-done | bytes 131104 | tf_op jit(solution)/shard_map/ppermute | solution.py:82
  218.0 3.2 %collective-permute-done.51 = bf16[256,256]{1,0:T(8,128)(2,1)S(1)} collective-permute-done((bf16[256,256]{1,0:T(8,128)(2,1)S(1)}, bf16[256,256]{1,0:T(8,128)(2,1)S(1)}, u32[]{:S(2)}, u32[]{:S(2)}) %collective-permute-start.51) | collective-permute-done | bytes 131104 | tf_op jit(solution)/shard_map/ppermute | solution.py:82
  222.7 2.4 %copy.17 = f32[128,1536]{1,0:T(8,128)} copy(f32[128,1536]{0,1:T(8,128)} %pad_maximum_fusion.8) | data formatting | bytes 1572864
  225.2 2.6 %shard_map.87 = bf16[512,2048]{1,0:T(8,128)(2,1)} custom-call(s32[6]{0:T(128)S(1)} %stack.27.at_ref, bf16[256,1536]{1,0:T(8,128)(2,1)S(1)} %pad_maximum_fusion.7.refs_0_, bf16[256,1536]{1,0:T(8,128)(2,1)} %collective-permute-done.49.refs_1_, bf16[256,512]{1,0:T(8,128)(2,1)S(1)} %pad_maximum_fusion.17.refs_2_, ...), custom_call_target="tpu_custom_call" | custom-call | flops 4194304 | bytes 4194304 | tf_op jit(solution)/shard_map/pallas_call | solution.py:65
  (165 shorter events, 65.5 us)
Async XLA Ops:
  10.5 15.9 %collective-permute-start = (bf16[128,384]{1,0:T(8,128)(2,1)}, bf16[128,384]{1,0:T(8,128)(2,1)S(1)}, u32[]{:S(2)}, u32[]{:S(2)}) collective-permute-start(bf16[128,384]{1,0:T(8,128)(2,1)} %get-tuple-element.20), channel_id=1, source_target_pairs={{0,2},{2,0},{4,6},{6,4},{8,10},{10,8},{12,14},{14,12},{16,18},{18,... | collective-permute-start | bytes 294920 | tf_op jit(solution)/shard_map/ppermute | solution.py:82
  12.5 16.6 %collective-permute-start.1 = (bf16[128,384]{1,0:T(8,128)(2,1)}, bf16[128,384]{1,0:T(8,128)(2,1)S(1)}, u32[]{:S(2)}, u32[]{:S(2)}) collective-permute-start(bf16[128,384]{1,0:T(8,128)(2,1)} %get-tuple-element.21), channel_id=1, source_target_pairs={{0,4},{2,6},{4,0},{6,2},{8,12},{10,14},{12,8},{14,10},{16,20},{18,... | collective-permute-start | bytes 294920 | tf_op jit(solution)/shard_map/ppermute | solution.py:82
  23.2 35.0 %collective-permute-start.12 = (bf16[384,768]{1,0:T(8,128)(2,1)}, bf16[384,768]{1,0:T(8,128)(2,1)}, u32[]{:S(2)}, u32[]{:S(2)}) collective-permute-start(bf16[384,768]{1,0:T(8,128)(2,1)} %shard_map.81.refs_1_), channel_id=1, source_target_pairs={{0,8},{2,10},{4,12},{6,14},{8,24},{10,26},{12,28},{14,30},{16,0},{... | collective-permute-start | bytes 1769480 | tf_op jit(solution)/shard_map/ppermute | solution.py:85
  25.9 63.4 %collective-permute-start.15 = (bf16[256,2048]{1,0:T(8,128)(2,1)}, bf16[256,2048]{1,0:T(8,128)(2,1)S(1)}, u32[]{:S(2)}, u32[]{:S(2)}) collective-permute-start(bf16[256,2048]{1,0:T(8,128)(2,1)} %constant_dynamic-slice_fusion.2), channel_id=1, source_target_pairs={{0,2},{2,0},{4,6},{6,4},{8,10},{10,8},{12,14},{14,12},{16,18},{18,... | collective-permute-start | bytes 3145736 | tf_op jit(solution)/shard_map/ppermute | solution.py:82
  26.4 20.5 %collective-permute-start.3 = (bf16[128,1152]{1,0:T(8,128)(2,1)}, bf16[128,1152]{1,0:T(8,128)(2,1)}, u32[]{:S(2)}, u32[]{:S(2)}) collective-permute-start(bf16[128,1152]{1,0:T(8,128)(2,1)} %get-tuple-element.19.refs_0_), channel_id=1, source_target_pairs={{0,8},{2,10},{4,12},{6,14},{8,24},{10,26},{12,28},{14,30},{16,0},{... | collective-permute-start | bytes 884744 | tf_op jit(solution)/shard_map/ppermute | solution.py:85
  31.1 22.2 %collective-permute-start.4 = (bf16[384,384]{1,0:T(8,128)(2,1)S(1)}, bf16[384,384]{1,0:T(8,128)(2,1)}, u32[]{:S(2)}, u32[]{:S(2)}) collective-permute-start(bf16[384,384]{1,0:T(8,128)(2,1)S(1)} %shard_map.78.refs_1_), channel_id=1, source_target_pairs={{0,8},{2,10},{4,12},{6,14},{8,24},{10,26},{12,28},{14,30},{16,0},{... | collective-permute-start | bytes 884744 | tf_op jit(solution)/shard_map/ppermute | solution.py:85
  54.0 39.6 %collective-permute-start.20 = (bf16[256,2048]{1,0:T(8,128)(2,1)}, bf16[256,2048]{1,0:T(8,128)(2,1)}, u32[]{:S(2)}, u32[]{:S(2)}) collective-permute-start(bf16[256,2048]{1,0:T(8,128)(2,1)} %constant_dynamic-slice_fusion.2), channel_id=1, source_target_pairs={{0,4},{2,6},{4,0},{6,2},{8,12},{10,14},{12,8},{14,10},{16,20},{18,... | collective-permute-start | bytes 3145736 | tf_op jit(solution)/shard_map/ppermute | solution.py:82
  58.2 31.1 %collective-permute-start.13 = (bf16[384,768]{1,0:T(8,128)(2,1)}, bf16[384,768]{1,0:T(8,128)(2,1)S(1)}, u32[]{:S(2)}, u32[]{:S(2)}) collective-permute-start(bf16[384,768]{1,0:T(8,128)(2,1)} %collective-permute-done.12.refs_3_), channel_id=1, source_target_pairs={{0,8},{2,10},{4,12},{6,14},{8,24},{10,26},{12,28},{14,30},{16,0},{... | collective-permute-start | bytes 1769480 | tf_op jit(solution)/shard_map/ppermute | solution.py:85
  61.8 22.8 %collective-permute-start.7 = (bf16[128,1152]{1,0:T(8,128)(2,1)}, bf16[128,1152]{1,0:T(8,128)(2,1)S(1)}, u32[]{:S(2)}, u32[]{:S(2)}) collective-permute-start(bf16[128,1152]{1,0:T(8,128)(2,1)} %collective-permute-done.5.refs_4_), channel_id=1, source_target_pairs={{0,8},{2,10},{4,12},{6,14},{8,24},{10,26},{12,28},{14,30},{16,0},{... | collective-permute-start | bytes 884744 | tf_op jit(solution)/shard_map/ppermute | solution.py:85
  65.9 21.9 %collective-permute-start.8 = (bf16[384,384]{1,0:T(8,128)(2,1)}, bf16[384,384]{1,0:T(8,128)(2,1)S(1)}, u32[]{:S(2)}, u32[]{:S(2)}) collective-permute-start(bf16[384,384]{1,0:T(8,128)(2,1)} %collective-permute-done.6.refs_5_), channel_id=1, source_target_pairs={{0,8},{2,10},{4,12},{6,14},{8,24},{10,26},{12,28},{14,30},{16,0},{... | collective-permute-start | bytes 884744 | tf_op jit(solution)/shard_map/ppermute | solution.py:85
  84.6 25.5 %collective-permute-start.17 = (bf16[512,768]{1,0:T(8,128)(2,1)S(1)}, bf16[512,768]{1,0:T(8,128)(2,1)S(1)}, u32[]{:S(2)}, u32[]{:S(2)}) collective-permute-start(bf16[512,768]{1,0:T(8,128)(2,1)S(1)} %get-tuple-element.27), channel_id=1, source_target_pairs={{0,2},{2,0},{4,6},{6,4},{8,10},{10,8},{12,14},{14,12},{16,18},{18,... | collective-permute-start | bytes 2359304 | tf_op jit(solution)/shard_map/ppermute | solution.py:82
  89.3 18.3 %collective-permute-start.16 = (bf16[256,2048]{1,0:T(8,128)(2,1)S(1)}, bf16[256,2048]{1,0:T(8,128)(2,1)S(1)}, u32[]{:S(2)}, u32[]{:S(2)}) collective-permute-start(bf16[256,2048]{1,0:T(8,128)(2,1)S(1)} %collective-permute-done.15.refs_0_), channel_id=1, source_target_pairs={{0,1},{1,0},{2,3},{3,2},{4,5},{5,4},{6,7},{7,6},{8,9},{9,8},{10,11... | collective-permute-start | bytes 3145736 | tf_op jit(solution)/shard_map/ppermute | solution.py:91
  89.4 16.6 %collective-permute-start.34 = (bf16[384,768]{1,0:T(8,128)(2,1)S(1)}, bf16[384,768]{1,0:T(8,128)(2,1)S(1)}, u32[]{:S(2)}, u32[]{:S(2)}) collective-permute-start(bf16[384,768]{1,0:T(8,128)(2,1)S(1)} %collective-permute-done.13.refs_5_), channel_id=1, source_target_pairs={{0,8},{2,10},{4,12},{6,14},{8,24},{10,26},{12,28},{14,30},{16,0},{... | collective-permute-start | bytes 1769480 | tf_op jit(solution)/shard_map/ppermute | solution.py:85
  93.2 17.0 %collective-permute-start.24 = (bf16[128,2048]{1,0:T(8,128)(2,1)S(1)}, bf16[128,2048]{1,0:T(8,128)(2,1)S(1)}, u32[]{:S(2)}, u32[]{:S(2)}) collective-permute-start(bf16[128,2048]{1,0:T(8,128)(2,1)S(1)} %slice.189), channel_id=1, source_target_pairs={{0,4},{2,6},{4,0},{6,2},{8,12},{10,14},{12,8},{14,10},{16,20},{18,... | collective-permute-start | bytes 1572872 | tf_op jit(solution)/shard_map/ppermute | solution.py:82
  94.7 16.0 %collective-permute-start.25 = (bf16[128,2048]{1,0:T(8,128)(2,1)S(1)}, bf16[128,2048]{1,0:T(8,128)(2,1)S(1)}, u32[]{:S(2)}, u32[]{:S(2)}) collective-permute-start(bf16[128,2048]{1,0:T(8,128)(2,1)S(1)} %slice.190), channel_id=1, source_target_pairs={{0,2},{2,0},{4,6},{6,4},{8,10},{10,8},{12,14},{14,12},{16,18},{18,... | collective-permute-start | bytes 1572872 | tf_op jit(solution)/shard_map/ppermute | solution.py:82
  106.0 35.7 %collective-permute-start.22 = (bf16[512,768]{1,0:T(8,128)(2,1)S(1)}, bf16[512,768]{1,0:T(8,128)(2,1)S(1)}, u32[]{:S(2)}, u32[]{:S(2)}) collective-permute-start(bf16[512,768]{1,0:T(8,128)(2,1)S(1)} %get-tuple-element.28), channel_id=1, source_target_pairs={{0,4},{2,6},{4,0},{6,2},{8,12},{10,14},{12,8},{14,10},{16,20},{18,... | collective-permute-start | bytes 2359304 | tf_op jit(solution)/shard_map/ppermute | solution.py:82
  107.6 35.2 %collective-permute-start.28 = (bf16[512,768]{1,0:T(8,128)(2,1)S(1)}, bf16[512,768]{1,0:T(8,128)(2,1)S(1)}, u32[]{:S(2)}, u32[]{:S(2)}) collective-permute-start(bf16[512,768]{1,0:T(8,128)(2,1)S(1)} %get-tuple-element.29), channel_id=1, source_target_pairs={{0,6},{2,4},{4,2},{6,0},{8,14},{10,12},{12,10},{14,8},{16,22},{18,... | collective-permute-start | bytes 2359304 | tf_op jit(solution)/shard_map/ppermute | solution.py:82
  114.3 42.3 %collective-permute-start.14 = (bf16[256,1536]{1,0:T(8,128)(2,1)S(1)}, bf16[256,1536]{1,0:T(8,128)(2,1)S(1)}, u32[]{:S(2)}, u32[]{:S(2)}) collective-permute-start(bf16[256,1536]{1,0:T(8,128)(2,1)S(1)} %slice.177), channel_id=1, source_target_pairs={{0,1},{1,0},{2,3},{3,2},{4,5},{5,4},{6,7},{7,6},{8,9},{9,8},{10,11... | collective-permute-start | bytes 2359304 | tf_op jit(solution)/shard_map/ppermute | solution.py:91
  116.2 40.7 %collective-permute-start.50 = (bf16[256,512]{1,0:T(8,128)(2,1)S(1)}, bf16[256,512]{1,0:T(8,128)(2,1)S(1)}, u32[]{:S(2)}, u32[]{:S(2)}) collective-permute-start(bf16[256,512]{1,0:T(8,128)(2,1)S(1)} %slice.211), channel_id=1, source_target_pairs={{0,1},{1,0},{2,3},{3,2},{4,5},{5,4},{6,7},{7,6},{8,9},{9,8},{10,11... | collective-permute-start | bytes 786440 | tf_op jit(solution)/shard_map/ppermute | solution.py:91
  146.8 26.0 %collective-permute-start.43 = (bf16[512,384]{0,1:T(8,128)(2,1)S(1)}, bf16[512,384]{0,1:T(8,128)(2,1)S(1)}, u32[]{:S(2)}, u32[]{:S(2)}) collective-permute-start(bf16[512,384]{0,1:T(8,128)(2,1)S(1)} %get-tuple-element.40), channel_id=1, source_target_pairs={{0,16},{2,18},{4,20},{6,22},{8,24},{10,26},{12,28},{14,30},{16,0},... | collective-permute-start | bytes 1179656 | tf_op jit(solution)/shard_map/ppermute | solution.py:88
  148.6 24.6 %collective-permute-start.44 = (bf16[512,384]{0,1:T(8,128)(2,1)S(1)}, bf16[512,384]{0,1:T(8,128)(2,1)S(1)}, u32[]{:S(2)}, u32[]{:S(2)}) collective-permute-start(bf16[512,384]{0,1:T(8,128)(2,1)S(1)} %get-tuple-element.39), channel_id=1, source_target_pairs={{0,24},{2,26},{4,28},{6,30},{8,0},{10,2},{12,4},{14,6},{16,8},{18,... | collective-permute-start | bytes 1179656 | tf_op jit(solution)/shard_map/ppermute | solution.py:88
  158.6 21.8 %collective-permute-start.18 = (bf16[256,1536]{1,0:T(8,128)(2,1)S(1)}, bf16[256,1536]{1,0:T(8,128)(2,1)S(1)}, u32[]{:S(2)}, u32[]{:S(2)}) collective-permute-start(bf16[256,1536]{1,0:T(8,128)(2,1)S(1)} %slice.182), channel_id=1, source_target_pairs={{0,1},{1,0},{2,3},{3,2},{4,5},{5,4},{6,7},{7,6},{8,9},{9,8},{10,11... | collective-permute-start | bytes 2359304 | tf_op jit(solution)/shard_map/ppermute | solution.py:91
  159.7 19.1 %collective-permute-start.29 = (bf16[256,1536]{1,0:T(8,128)(2,1)S(1)}, bf16[256,1536]{1,0:T(8,128)(2,1)S(1)}, u32[]{:S(2)}, u32[]{:S(2)}) collective-permute-start(bf16[256,1536]{1,0:T(8,128)(2,1)S(1)} %slice.194), channel_id=1, source_target_pairs={{0,1},{1,0},{2,3},{3,2},{4,5},{5,4},{6,7},{7,6},{8,9},{9,8},{10,11... | collective-permute-start | bytes 2359304 | tf_op jit(solution)/shard_map/ppermute | solution.py:91
  159.9 21.5 %collective-permute-start.23 = (bf16[256,1536]{1,0:T(8,128)(2,1)S(1)}, bf16[256,1536]{1,0:T(8,128)(2,1)S(1)}, u32[]{:S(2)}, u32[]{:S(2)}) collective-permute-start(bf16[256,1536]{1,0:T(8,128)(2,1)S(1)} %slice.187), channel_id=1, source_target_pairs={{0,1},{1,0},{2,3},{3,2},{4,5},{5,4},{6,7},{7,6},{8,9},{9,8},{10,11... | collective-permute-start | bytes 2359304 | tf_op jit(solution)/shard_map/ppermute | solution.py:91
  173.2 20.6 %collective-permute-start.37 = (bf16[256,256]{1,0:T(8,128)(2,1)S(1)}, bf16[256,256]{1,0:T(8,128)(2,1)S(1)}, u32[]{:S(2)}, u32[]{:S(2)}) collective-permute-start(bf16[256,256]{1,0:T(8,128)(2,1)S(1)} %get-tuple-element.62), channel_id=1, source_target_pairs={{0,2},{2,0},{4,6},{6,4},{8,10},{10,8},{12,14},{14,12},{16,18},{18,... | collective-permute-start | bytes 393224 | tf_op jit(solution)/shard_map/ppermute | solution.py:82
  178.2 16.9 %collective-permute-start.45 = (bf16[128,384]{0,1:T(8,128)(2,1)S(1)}, bf16[128,384]{0,1:T(8,128)(2,1)S(1)}, u32[]{:S(2)}, u32[]{:S(2)}) collective-permute-start(bf16[128,384]{0,1:T(8,128)(2,1)S(1)} %get-tuple-element.51), channel_id=1, source_target_pairs={{0,2},{2,0},{4,6},{6,4},{8,10},{10,8},{12,14},{14,12},{16,18},{18,... | collective-permute-start | bytes 294920 | tf_op jit(solution)/shard_map/ppermute | solution.py:82
  178.8 17.3 %collective-permute-start.46 = (bf16[128,384]{0,1:T(8,128)(2,1)S(1)}, bf16[128,384]{0,1:T(8,128)(2,1)S(1)}, u32[]{:S(2)}, u32[]{:S(2)}) collective-permute-start(bf16[128,384]{0,1:T(8,128)(2,1)S(1)} %get-tuple-element.53), channel_id=1, source_target_pairs={{0,4},{2,6},{4,0},{6,2},{8,12},{10,14},{12,8},{14,10},{16,20},{18,... | collective-permute-start | bytes 294920 | tf_op jit(solution)/shard_map/ppermute | solution.py:82
  193.8 23.8 %collective-permute-start.19 = (bf16[256,768]{1,0:T(8,128)(2,1)S(1)}, bf16[256,768]{1,0:T(8,128)(2,1)S(1)}, u32[]{:S(2)}, u32[]{:S(2)}) collective-permute-start(bf16[256,768]{1,0:T(8,128)(2,1)S(1)} %slice.305), channel_id=1, source_target_pairs={{0,2},{2,0},{4,6},{6,4},{8,10},{10,8},{12,14},{14,12},{16,18},{18,... | collective-permute-start | bytes 1179656 | tf_op jit(solution)/shard_map/ppermute | solution.py:82
  195.1 22.5 %collective-permute-start.48 = (bf16[256,768]{1,0:T(8,128)(2,1)S(1)}, bf16[256,768]{1,0:T(8,128)(2,1)S(1)}, u32[]{:S(2)}, u32[]{:S(2)}) collective-permute-start(bf16[256,768]{1,0:T(8,128)(2,1)S(1)} %slice.304), channel_id=1, source_target_pairs={{0,4},{2,6},{4,0},{6,2},{8,12},{10,14},{12,8},{14,10},{16,20},{18,... | collective-permute-start | bytes 1179656 | tf_op jit(solution)/shard_map/ppermute | solution.py:82
  196.1 20.5 %collective-permute-start.33 = (bf16[256,768]{1,0:T(8,128)(2,1)S(1)}, bf16[256,768]{1,0:T(8,128)(2,1)S(1)}, u32[]{:S(2)}, u32[]{:S(2)}) collective-permute-start(bf16[256,768]{1,0:T(8,128)(2,1)S(1)} %fusion.44), channel_id=1, source_target_pairs={{0,2},{2,0},{4,6},{6,4},{8,10},{10,8},{12,14},{14,12},{16,18},{18,... | collective-permute-start | bytes 1179656 | tf_op jit(solution)/shard_map/ppermute | solution.py:82
  197.6 20.0 %collective-permute-start.31 = (bf16[256,768]{1,0:T(8,128)(2,1)S(1)}, bf16[256,768]{1,0:T(8,128)(2,1)S(1)}, u32[]{:S(2)}, u32[]{:S(2)}) collective-permute-start(bf16[256,768]{1,0:T(8,128)(2,1)S(1)} %fusion.45), channel_id=1, source_target_pairs={{0,4},{2,6},{4,0},{6,2},{8,12},{10,14},{12,8},{14,10},{16,20},{18,... | collective-permute-start | bytes 1179656 | tf_op jit(solution)/shard_map/ppermute | solution.py:82
  199.9 16.2 %collective-permute-start.38 = (bf16[256,256]{1,0:T(8,128)(2,1)S(1)}, bf16[256,256]{1,0:T(8,128)(2,1)S(1)}, u32[]{:S(2)}, u32[]{:S(2)}) collective-permute-start(bf16[256,256]{1,0:T(8,128)(2,1)S(1)} %fusion.74), channel_id=1, source_target_pairs={{0,4},{2,6},{4,0},{6,2},{8,12},{10,14},{12,8},{14,10},{16,20},{18,... | collective-permute-start | bytes 393224 | tf_op jit(solution)/shard_map/ppermute | solution.py:82
  (32 other events, 210.7 us)
where the time goes:
time: 232 us; the launch traced here: 228 us
  waiting for transfers between devices  124 us (53%)
  starting transfers between devices  51.6 us (22%)
  matrix products  21.1 us (9%)
  local copies, waits for them, and re-layouts  13.6 us (6%)
  Pallas kernels  13.3 us (6%)
  other arithmetic  3.13 us (1%)
    ppermute x28, waiting for transfers between devices, xperm(): lax.ppermute(v, 'fs', [(j, j // B * B + (j % B ^ k)) for j in range(n)])  60.2 us
    ppermute x9, waiting for transfers between devices, zring(): lax.ppermute(v, 'fs', [(j, after[j // B] * B + j % B) for j in range(n)])  49.5 us
    ppermute x28, starting transfers between devices, xperm(): lax.ppermute(v, 'fs', [(j, j // B * B + (j % B ^ k)) for j in range(n)])  31.8 us
    pallas_call x11, Pallas kernels, packed(): pl.pallas_call(kernel, in_specs=[pl.BlockSpec(memory_space=pltpu.SMEM)] +...  13.3 us
    ppermute x3, waiting for transfers between devices, zshift(): lax.ppermute(v, 'fs', [(j, (j // B + s) % a * B + j % B) for j in range(n)])  12.5 us
    ppermute x9, starting transfers between devices, zring(): lax.ppermute(v, 'fs', [(j, after[j // B] * B + j % B) for j in range(n)])  11.7 us
    unnamed x21, local copies, waits for them, and re-layouts  10.5 us
    dot_general x8, matrix products, local(): lax.dot_general(dgus[k], wgu, (((1,), (1,)), ((), ())), preferred_element...  8.1 us
  transfers between devices with their start and end apart: 54, of which 19 were waited for; matrix products, arithmetic and copies ran while one was open for 13% of the time, Pallas kernels for 4%

commit v1 on v0

--- a/solution.py
+++ b/solution.py
@@ -12,14 +12,12 @@
 B = 4
 
 
-def pack_weights_kernel(fb, at_ref, d_ref, g_ref, u_ref, own_ref, *outs):
+def pack_weights_kernel(fb, at_ref, d_ref, g_ref, u_ref, *outs):
     for k in range(B):
         at = pl.ds(pl.multiple_of((at_ref[0] ^ k) * fb, 128), fb)
-        d, gu = (outs[k - 1], outs[B + k - 2]) if k else (own_ref, own_ref)
-        first = 0 if k else fb
-        d[:, :fb] = d_ref[:, at]
-        gu[:, first : first + fb] = g_ref[:, at]
-        gu[:, first + fb : first + 2 * fb] = u_ref[:, at]
+        outs[k][:, :fb] = d_ref[:, at]
+        outs[k][:, fb : 2 * fb] = g_ref[:, at]
+        outs[k][:, 2 * fb :] = u_ref[:, at]
 
 
 def pack_tokens_kernel(fb, rows, tp, at_ref, g_ref, u_ref, *outs):
@@ -42,32 +40,79 @@
             out_ref[pl.ds(row, wrows), :] = v
 
 
-def stack_kernel(at_ref, *refs):
-    *pieces, out_ref = refs
+def stack_kernel(cuts, at_ref, *refs):
+    pieces, outs = refs[: -len(cuts)], refs[-len(cuts) :]
     row = 0
     for v in pieces:
-        out_ref[row : row + v.shape[0], :] = v[...]
+        for (lo, hi), out_ref in zip(cuts, outs):
+            out_ref[row : row + v.shape[0], :] = v[:, lo:hi]
         row += v.shape[0]
 
 
-def result_kernel(rows, at_ref, *refs):
-    *pieces, out_ref = refs
-    for v, (h, t, lo, width) in zip(pieces, rows[1]):
-        here = pl.ds(pl.multiple_of((at_ref[1] ^ h) * rows[0], 16), rows[0])
+def place_kernel(rows, places, at_ref, *refs):
+    *pieces, out_ref, sems = refs
+    copies = []
+    for v, (h, t, width) in zip(pieces, places):
+        here = pl.ds(pl.multiple_of((at_ref[1] ^ h) * rows, 16), rows)
         for j in range(v.shape[1] // width):
             there = pl.ds(pl.multiple_of(at_ref[2 + t + j] * width, 128), width)
-            out_ref[here, there] = v[:, j * width : (j + 1) * width]
-
-
-def packed(kernel, at, arrays, shapes):
+            target = out_ref.at[here, there]
+            source = v.at[:, j * width : (j + 1) * width]
+            copies.append(pltpu.make_async_copy(source, target, sems.at[len(copies)]))
+            copies[-1].start()
+    for copy in copies:
+        copy.wait()
+
+
+def placed_blocks(rows, places, at, pieces, shape):
+    steps = sum(v.shape[1] // width for v, (_, _, width) in zip(pieces, places))
+    inside = pl.BlockSpec(memory_space=pltpu.VMEM)
+    moved = 4 * shape[0] * shape[1]
+    return pl.pallas_call(
+        functools.partial(place_kernel, rows, places),
+        in_specs=[pl.BlockSpec(memory_space=pltpu.SMEM)] + [inside] * len(pieces),
+        out_specs=pl.BlockSpec(memory_space=pl.ANY),
+        out_shape=jax.ShapeDtypeStruct(shape, BF16),
+        scratch_shapes=[pltpu.SemaphoreType.DMA((steps,))],
+        compiler_params=pltpu.CompilerParams(vmem_limit_bytes=moved + (3 << 20)),
+        cost_estimate=pl.CostEstimate(flops=moved, bytes_accessed=moved, transcendentals=0),
+    )(at, *pieces)
+
+
+def turn_copy_kernel(fb, at_ref, *refs):
+    pieces, out_ref, held, sems = refs[:B], refs[B], refs[B + 1 : -1], refs[-1]
+    copies = [pltpu.make_async_copy(v, h, sems.at[k]) for k, (v, h) in enumerate(zip(pieces, held))]
+    for copy in copies:
+        copy.start()
+    for k in range(B):
+        copies[k].wait()
+        there = pl.ds(pl.multiple_of((at_ref[0] ^ k) * fb, 128), fb)
+        out_ref[:, there] = held[k][...].astype(F32).T
+
+
+def turned(fb, at, pieces, shape):
+    moved = 8 * shape[0] * shape[1]
+    return pl.pallas_call(
+        functools.partial(turn_copy_kernel, fb),
+        in_specs=[pl.BlockSpec(memory_space=pltpu.SMEM)] + [pl.BlockSpec(memory_space=pl.ANY)] * B,
+        out_specs=pl.BlockSpec(),
+        out_shape=jax.ShapeDtypeStruct(shape, F32),
+        scratch_shapes=[pltpu.VMEM(v.shape, v.dtype) for v in pieces] + [pltpu.SemaphoreType.DMA((B,))],
+        compiler_params=pltpu.CompilerParams(vmem_limit_bytes=moved + (3 << 20)),
+        cost_estimate=pl.CostEstimate(flops=moved, bytes_accessed=moved, transcendentals=0),
+    )(at, *pieces)
+
+
+def packed(kernel, at, arrays, shapes, dtype=BF16, limit=True):
     whole = pl.BlockSpec()
+    inside = pl.BlockSpec(memory_space=pltpu.VMEM) if limit == 2 else whole
     moved = 2 * sum(v.size for v in arrays) + 2 * sum(math.prod(x) for x in shapes)
     return pl.pallas_call(
         kernel,
-        in_specs=[pl.BlockSpec(memory_space=pltpu.SMEM)] + [whole] * len(arrays),
+        in_specs=[pl.BlockSpec(memory_space=pltpu.SMEM)] + [inside] * len(arrays),
         out_specs=[whole] * len(shapes),
-        out_shape=[jax.ShapeDtypeStruct(s, BF16) for s in shapes],
-        compiler_params=pltpu.CompilerParams(vmem_limit_bytes=moved + (2 << 20)),
+        out_shape=[jax.ShapeDtypeStruct(s, dtype) for s in shapes],
+        compiler_params=pltpu.CompilerParams(vmem_limit_bytes=moved + (3 << 20) if limit else None),
         cost_estimate=pl.CostEstimate(flops=moved, bytes_accessed=moved, transcendentals=0),
     )(at, *arrays)
 
@@ -120,28 +165,30 @@
 
         tiled = fb % 128 == 0 and wrows % 16 == 0 and zrows % 128 == 0 and half % 32 == 0
 
-        def stacked(got):
+        def stacked(got, *cuts):
             if not tiled:
-                return jnp.concatenate(got, 0)
-            return packed(stack_kernel, at, got, [(sum(v.shape[0] for v in got), got[0].shape[1])])[0]
+                return [jnp.concatenate(got, 0)[:, lo:hi] for lo, hi in cuts]
+            rows = sum(v.shape[0] for v in got)
+            kernel = functools.partial(stack_kernel, cuts)
+            return packed(kernel, at, got, [(rows, hi - lo) for lo, hi in cuts])
 
         if tiled:
             packs = packed(
                 functools.partial(pack_weights_kernel, fb),
                 at,
                 (wd, wg, wu),
-                [(wrows, 3 * fb)] + [(wrows, fb)] * (B - 1) + [(wrows, 2 * fb)] * (B - 1),
+                [(wrows, 3 * fb)] * B,
+                limit=0,
             )
             tok = packed(
                 functools.partial(pack_tokens_kernel, fb, half, tp),
                 at,
                 (g, u),
                 [(tokens, 2 * fb)] * B,
+                limit=1,
             )
         else:
-            packs = [jnp.concatenate([cols(wd, q), cols(wg, q), cols(wu, q)], 1)]
-            packs += [cols(wd, q ^ k) for k in range(1, B)]
-            packs += [jnp.concatenate([cols(wg, q ^ k), cols(wu, q ^ k)], 1) for k in range(1, B)]
+            packs = [jnp.concatenate([cols(v, q ^ k) for v in (wd, wg, wu)], 1) for k in range(B)]
             tok = [
                 jnp.concatenate(
                     [jnp.concatenate([cols(part(v, h), q ^ k) for h in range(tp)], 0) for v in (g, u)], 1
@@ -150,8 +197,8 @@
             ]
 
         ros = [packs[0]]
-        rds = [stacked([xperm(packs[k], k) for k in range(1, B)])]
-        rgs = [stacked([xperm(packs[B - 1 + k], k) for k in range(1, B)])]
+        got = [xperm(packs[k], k) for k in range(1, B)]
+        rds, rgs = [[v] for v in stacked(got, (0, fb), (fb, 3 * fb))]
         for _ in range(1, a):
             ros.append(zring(ros[-1]))
             rds.append(zring(rds[-1]))
@@ -183,7 +230,7 @@
         cots = [jnp.concatenate([mine] + [part(own, h) for h in range(1, tp)], 0)]
         for got in ([m1], [m2], m3):
             swapped = [tperm(v, h) for h in range(1, tp) for v in got]
-            cots.append(stacked(got + swapped))
+            cots.append(stacked(got + swapped, (0, width))[0])
         gus = [tok[0]] + [xperm(tok[k], k) for k in range(1, B)]
 
         down = None
@@ -198,19 +245,24 @@
             d_up = (dh * gate * sigma).astype(BF16)
             dgus.append(jnp.concatenate([d_gate, d_up], 1))
             term = lax.dot_general(
-                cots[k], hidden, (((0,), (0,)), ((), ())), preferred_element_type=F32
+                hidden, cots[k], (((0,), (0,)), ((), ())), preferred_element_type=F32
             )
             down = term if down is None else down + term
 
-        acc = lax.dynamic_slice_in_dim(down, z * zrows, zrows, 0)
+        acc = lax.dynamic_slice_in_dim(down, z * zrows, zrows, 1)
         for s in range(1, a):
-            sent = lax.dynamic_slice_in_dim(down, ((z + s) % a) * zrows, zrows, 0).astype(BF16)
+            sent = lax.dynamic_slice_in_dim(down, ((z + s) % a) * zrows, zrows, 1).astype(BF16)
             acc = acc + zshift(sent, s).astype(F32)
         got = []
         for k in range(B):
-            v = lax.dynamic_slice_in_dim(acc, (q ^ k) * wrows, wrows, 0)
-            got.append(xperm(v.astype(BF16), k).astype(F32) if k else v)
-        grad_down = jnp.concatenate([lax.select_n(q ^ r, *got) for r in range(B)], 1)
+            v = lax.dynamic_slice_in_dim(acc, (q ^ k) * wrows, wrows, 1)
+            got.append(xperm(v.astype(BF16), k) if k else v)
+        if tiled:
+            grad_down = turned(fb, at, got, (wrows, B * fb))
+        else:
+            grad_down = jnp.concatenate(
+                [lax.select_n(q ^ r, *[v.astype(F32) for v in got]).T for r in range(B)], 1
+            )
 
         chunks = [(0, a - 1), (a - 1, a)] if a > 1 else [(0, 1)]
         finished = []
@@ -218,7 +270,9 @@
             wgu = assembled(range(t0, t1), rgs, fb, 3 * fb, False)
             sums = [None] * B
             for k in (1, 2, 3, 0):
-                gi = lax.dot_general(dgus[k], wgu, (((1,), (1,)), ((), ())), preferred_element_type=F32).astype(BF16)
+                gi = lax.dot_general(
+                    dgus[k], wgu, (((1,), (1,)), ((), ())), preferred_element_type=F32
+                ).astype(BF16)
                 s = gi[:half].astype(F32)
                 for h in range(1, tp):
                     s = s + tperm(gi[h * half : (h + 1) * half], h).astype(F32)
@@ -231,19 +285,17 @@
                 relay = (sums[second][:, lo:hi] + onward).astype(BF16)
                 outs.append((sums[0][:, lo:hi] + direct, xperm(relay, second)))
             finished.append(outs)
-        flat = lax.optimization_barrier(([r for outs in finished for _, r in outs], got))[0]
         pieces, places = [], []
-        for (t0, t1), outs, late in zip(chunks, finished, [flat[j : j + 2] for j in range(0, len(flat), 2)]):
-            own = jnp.concatenate([s + r.astype(F32) for (s, _), r in zip(outs, late)], 1).astype(BF16)
+        for (t0, t1), outs in zip(chunks, finished):
+            own = jnp.concatenate([s + r.astype(F32) for s, r in outs], 1).astype(BF16)
             pieces.append(own)
             places.append((0, t0, 0, zrows))
             for h in range(1, tp):
                 pieces.append(tperm(own, h))
                 places.append((h, t0, 0, zrows))
         if tiled:
-            grad_input = packed(
-                functools.partial(result_kernel, (half, tuple(places))), at, pieces, [(tokens, width)]
-            )[0]
+            spots = tuple((h, t, w) for h, t, _, w in places)
+            grad_input = placed_blocks(half, spots, at, pieces, (tokens, width))
         else:
             grad_input = jnp.zeros((tokens, width), BF16)
             for v, (h, t, _, wide) in zip(pieces, places):

time: 232 us -> 218 us (0.940)
  the two profiles are of different devices: /device:TPU:0 before, /device:TPU:10 now
where the time goes in v1:
time: 218 us
  waiting for transfers between devices  120 us (55%)
  starting transfers between devices  50.1 us (23%)
  matrix products  21.2 us (10%)
  Pallas kernels  15.3 us (7%)
  local copies, waits for them, and re-layouts  7.07 us (3%)
    ppermute x25, waiting for transfers between devices, xperm(): lax.ppermute(v, 'fs', [(j, j // B * B + (j % B ^ k)) for j in range(n)])  62.5 us
    ppermute x9, waiting for transfers between devices, zring(): lax.ppermute(v, 'fs', [(j, after[j // B] * B + j % B) for j in range(n)])  41.9 us
    ppermute x25, starting transfers between devices, xperm(): lax.ppermute(v, 'fs', [(j, j // B * B + (j % B ^ k)) for j in range(n)])  25 us
    ppermute x9, starting transfers between devices, zring(): lax.ppermute(v, 'fs', [(j, after[j // B] * B + j % B) for j in range(n)])  19.8 us
    ppermute x3, waiting for transfers between devices, zshift(): lax.ppermute(v, 'fs', [(j, (j // B + s) % a * B + j % B) for j in range(n)])  15.5 us
    pallas_call x9, Pallas kernels, packed(): pl.pallas_call(kernel, in_specs=[pl.BlockSpec(memory_space=pltpu.SMEM)] +...  10.9 us
    dot_general x8, matrix products, local(): lax.dot_general(dgus[k], wgu, (((1,), (1,)), ((), ())), preferred_element...  8.15 us
    dot_general x4, matrix products, local(): dh = jnp.dot(cots[k], wd_full, preferred_element_type=F32)  7.08 us
  transfers between devices with their start and end apart: 51, of which 24 were waited for; matrix products, arithmetic and copies ran while one was open for 12% of the time, Pallas kernels for 4%

profile of v1, /device:TPU:10, one launch (start us, length us, event | category | flops | bytes accessed | tf_op | source)
XLA Modules:
  0.0 217.8 jit_solution(14641281728920017192)
XLA Ops:
  1.4 2.4 %shard_map.77 = (bf16[128,1152]{1,0:T(8,128)(2,1)}, bf16[128,1152]{1,0:T(8,128)(2,1)}, bf16[128,1152]{1,0:T(8,128)(2,1)}, bf16[128,1152]{1,0:T(8,128)(2,1)}) custom-call(s32[6]{0:T(128)} %stack.27.at_ref, bf16[128,1536]{1,0:T(8,128)(2,1)} %d_ref.1, bf16[128,1536]{1,0:T(8,128)(2,1)} %g_ref.2, bf16[128,1536]{1,0:T(8,128)(2,1)} %u_ref.2), custom_call_target="tpu_custom_call" | custom-call | flops 2359296 | bytes 2359296 | tf_op jit(solution)/shard_map/pallas_call | solution.py:110
  7.2 6.6 %collective-permute-done.refs_0_ = bf16[128,1152]{1,0:T(8,128)(2,1)S(1)} collective-permute-done((bf16[128,1152]{1,0:T(8,128)(2,1)}, bf16[128,1152]{1,0:T(8,128)(2,1)S(1)}, u32[]{:S(2)}, u32[]{:S(2)}) %collective-permute-start) | collective-permute-done | bytes 294944 | tf_op jit(solution)/shard_map/ppermute | solution.py:127
  13.8 4.6 %collective-permute-done.1.refs_1_ = bf16[128,1152]{1,0:T(8,128)(2,1)S(1)} collective-permute-done((bf16[128,1152]{1,0:T(8,128)(2,1)}, bf16[128,1152]{1,0:T(8,128)(2,1)S(1)}, u32[]{:S(2)}, u32[]{:S(2)}) %collective-permute-start.1) | collective-permute-done | bytes 294944 | tf_op jit(solution)/shard_map/ppermute | solution.py:127
  22.0 2.6 %collective-permute-start.9 = (bf16[384,768]{1,0:T(8,128)(2,1)}, bf16[384,768]{1,0:T(8,128)(2,1)}, u32[]{:S(2)}, u32[]{:S(2)}) collective-permute-start(bf16[384,768]{1,0:T(8,128)(2,1)} %get-tuple-element.20.refs_1_), channel_id=1, source_target_pairs={{0,8},{2,10},{4,12},{6,14},{8,24},{10,26},{12,28},{14,30},{16,0},{... | collective-permute-start | bytes 1769480 | tf_op jit(solution)/shard_map/ppermute | solution.py:130
  28.8 16.1 %collective-permute-done.3.refs_2_ = bf16[128,1152]{1,0:T(8,128)(2,1)} collective-permute-done((bf16[128,1152]{1,0:T(8,128)(2,1)S(1)}, bf16[128,1152]{1,0:T(8,128)(2,1)}, u32[]{:S(2)}, u32[]{:S(2)}) %collective-permute-start.3) | collective-permute-done | bytes 294944 | tf_op jit(solution)/shard_map/ppermute | solution.py:130
  44.8 3.5 %collective-permute-start.5 = (bf16[128,1152]{1,0:T(8,128)(2,1)}, bf16[128,1152]{1,0:T(8,128)(2,1)}, u32[]{:S(2)}, u32[]{:S(2)}) collective-permute-start(bf16[128,1152]{1,0:T(8,128)(2,1)} %collective-permute-done.3.refs_2_), channel_id=1, source_target_pairs={{0,8},{2,10},{4,12},{6,14},{8,24},{10,26},{12,28},{14,30},{16,0},{... | collective-permute-start | bytes 884744 | tf_op jit(solution)/shard_map/ppermute | solution.py:130
  48.3 2.8 %collective-permute-done.4.refs_3_ = bf16[384,384]{1,0:T(8,128)(2,1)} collective-permute-done((bf16[384,384]{1,0:T(8,128)(2,1)S(1)}, bf16[384,384]{1,0:T(8,128)(2,1)}, u32[]{:S(2)}, u32[]{:S(2)}) %collective-permute-start.4) | collective-permute-done | bytes 294944 | tf_op jit(solution)/shard_map/ppermute | solution.py:130
  51.1 3.5 %collective-permute-start.6 = (bf16[384,384]{1,0:T(8,128)(2,1)}, bf16[384,384]{1,0:T(8,128)(2,1)}, u32[]{:S(2)}, u32[]{:S(2)}) collective-permute-start(bf16[384,384]{1,0:T(8,128)(2,1)} %collective-permute-done.4.refs_3_), channel_id=1, source_target_pairs={{0,8},{2,10},{4,12},{6,14},{8,24},{10,26},{12,28},{14,30},{16,0},{... | collective-permute-start | bytes 884744 | tf_op jit(solution)/shard_map/ppermute | solution.py:130
  58.4 2.5 %collective-permute-start.7 = (bf16[128,1152]{1,0:T(8,128)(2,1)}, bf16[128,1152]{1,0:T(8,128)(2,1)S(1)}, u32[]{:S(2)}, u32[]{:S(2)}) collective-permute-start(bf16[128,1152]{1,0:T(8,128)(2,1)} %collective-permute-done.5.refs_4_), channel_id=1, source_target_pairs={{0,8},{2,10},{4,12},{6,14},{8,24},{10,26},{12,28},{14,30},{16,0},{... | collective-permute-start | bytes 884744 | tf_op jit(solution)/shard_map/ppermute | solution.py:130
  60.9 2.9 %collective-permute-done.6.refs_5_ = bf16[384,384]{1,0:T(8,128)(2,1)} collective-permute-done((bf16[384,384]{1,0:T(8,128)(2,1)}, bf16[384,384]{1,0:T(8,128)(2,1)}, u32[]{:S(2)}, u32[]{:S(2)}) %collective-permute-start.6) | collective-permute-done | bytes 294944 | tf_op jit(solution)/shard_map/ppermute | solution.py:130
  63.9 3.4 %collective-permute-start.8 = (bf16[384,384]{1,0:T(8,128)(2,1)}, bf16[384,384]{1,0:T(8,128)(2,1)S(1)}, u32[]{:S(2)}, u32[]{:S(2)}) collective-permute-start(bf16[384,384]{1,0:T(8,128)(2,1)} %collective-permute-done.6.refs_5_), channel_id=1, source_target_pairs={{0,8},{2,10},{4,12},{6,14},{8,24},{10,26},{12,28},{14,30},{16,0},{... | collective-permute-start | bytes 884744 | tf_op jit(solution)/shard_map/ppermute | solution.py:130
  67.3 2.3 %fusion = f32[384,2048]{1,0:T(8,128)S(1)} fusion(bf16[256,2048]{1,0:T(8,128)(2,1)S(1)} %constant_dynamic-slice_fusion.1, bf16[256,2048]{1,0:T(8,128)(2,1)} %constant_dynamic-slice_fusion.2, bf16[512,768]{1,0:T(8,128)(2,1)S(1)} %get-tuple-element.19), kind=kOutput, calls=%fused_computation.26 | convolution fusion | flops 811073536 | bytes 6029312 | tf_op jit(solution)/shard_map/dot_general | solution.py:247
  71.6 1.6 collective-permute-start.21
  73.2 9.7 %collective-permute-done.7.refs_6_.refs_0_ = bf16[128,1152]{1,0:T(8,128)(2,1)S(1)} collective-permute-done((bf16[128,1152]{1,0:T(8,128)(2,1)}, bf16[128,1152]{1,0:T(8,128)(2,1)S(1)}, u32[]{:S(2)}, u32[]{:S(2)}) %collective-permute-start.7) | collective-permute-done | bytes 294944 | tf_op jit(solution)/shard_map/ppermute | solution.py:130
  83.6 3.5 %collective-permute-done.8.refs_7_ = bf16[384,384]{1,0:T(8,128)(2,1)S(1)} collective-permute-done((bf16[384,384]{1,0:T(8,128)(2,1)}, bf16[384,384]{1,0:T(8,128)(2,1)S(1)}, u32[]{:S(2)}, u32[]{:S(2)}) %collective-permute-start.8) | collective-permute-done | bytes 294944 | tf_op jit(solution)/shard_map/ppermute | solution.py:130
  88.6 3.5 %collective-permute-start.33 = (bf16[384,768]{1,0:T(8,128)(2,1)S(1)}, bf16[384,768]{1,0:T(8,128)(2,1)S(1)}, u32[]{:S(2)}, u32[]{:S(2)}) collective-permute-start(bf16[384,768]{1,0:T(8,128)(2,1)S(1)} %collective-permute-done.10.refs_5_), channel_id=1, source_target_pairs={{0,8},{2,10},{4,12},{6,14},{8,24},{10,26},{12,28},{14,30},{16,0},{... | collective-permute-start | bytes 1769480 | tf_op jit(solution)/shard_map/ppermute | solution.py:130
  92.1 2.7 %fusion.4 = (bf16[512,384]{1,0:T(8,128)(2,1)S(1)}, bf16[512,384]{1,0:T(8,128)(2,1)S(1)}) fusion(bf16[512,768]{1,0:T(8,128)(2,1)S(1)} %get-tuple-element.19, bf16[2048,384]{1,0:T(8,128)(2,1)S(1)} %shard_map.79, bf16[256,2048]{1,0:T(8,128)(2,1)S(1)} %constant_dynamic-slice_fusion.1, bf16[256,2048]{1,0:T(8,128)(2,1)} %constant_dynamic-slice_fusion.2), kind=kOutput, calls=%fused_computation.42 | convolution fusion | flops 812449792 | bytes 5242880 | tf_op jit(solution)/shard_map/dot_general | solution.py:243
  98.5 6.9 %collective-permute-done.33.refs_1_ = bf16[384,768]{1,0:T(8,128)(2,1)S(1)} collective-permute-done((bf16[384,768]{1,0:T(8,128)(2,1)S(1)}, bf16[384,768]{1,0:T(8,128)(2,1)S(1)}, u32[]{:S(2)}, u32[]{:S(2)}) %collective-permute-start.33) | collective-permute-done | bytes 589856 | tf_op jit(solution)/shard_map/ppermute | solution.py:130
  112.3 6.3 %collective-permute-done.25 = bf16[512,768]{1,0:T(8,128)(2,1)S(1)} collective-permute-done((bf16[512,768]{1,0:T(8,128)(2,1)S(1)}, bf16[512,768]{1,0:T(8,128)(2,1)S(1)}, u32[]{:S(2)}, u32[]{:S(2)}) %collective-permute-start.25) | collective-permute-done | bytes 786464 | tf_op jit(solution)/shard_map/ppermute | solution.py:127
  124.3 11.1 %collective-permute-done.19 = bf16[512,768]{1,0:T(8,128)(2,1)S(1)} collective-permute-done((bf16[512,768]{1,0:T(8,128)(2,1)S(1)}, bf16[512,768]{1,0:T(8,128)(2,1)S(1)}, u32[]{:S(2)}, u32[]{:S(2)}) %collective-permute-start.19) | collective-permute-done | bytes 786464 | tf_op jit(solution)/shard_map/ppermute | solution.py:127
  151.3 8.0 %collective-permute-done.30 = bf16[256,768]{1,0:T(8,128)(2,1)S(1)} collective-permute-done((bf16[256,768]{1,0:T(8,128)(2,1)S(1)}, bf16[256,768]{1,0:T(8,128)(2,1)S(1)}, u32[]{:S(2)}, u32[]{:S(2)}) %collective-permute-start.30) | collective-permute-done | bytes 393248 | tf_op jit(solution)/shard_map/ppermute | solution.py:127
  160.0 8.2 %collective-permute-done.27 = bf16[256,768]{1,0:T(8,128)(2,1)S(1)} collective-permute-done((bf16[256,768]{1,0:T(8,128)(2,1)S(1)}, bf16[256,768]{1,0:T(8,128)(2,1)S(1)}, u32[]{:S(2)}, u32[]{:S(2)}) %collective-permute-start.27) | collective-permute-done | bytes 393248 | tf_op jit(solution)/shard_map/ppermute | solution.py:127
  173.0 5.1 %collective-permute-done.31 = bf16[256,768]{1,0:T(8,128)(2,1)S(1)} collective-permute-done((bf16[256,768]{1,0:T(8,128)(2,1)S(1)}, bf16[256,768]{1,0:T(8,128)(2,1)S(1)}, u32[]{:S(2)}, u32[]{:S(2)}) %collective-permute-start.31) | collective-permute-done | bytes 393248 | tf_op jit(solution)/shard_map/ppermute | solution.py:127
  178.6 1.8 collective-permute-start.41
  180.6 2.7 %collective-permute-done.36 = bf16[256,256]{1,0:T(8,128)(2,1)S(1)} collective-permute-done((bf16[256,256]{1,0:T(8,128)(2,1)S(1)}, bf16[256,256]{1,0:T(8,128)(2,1)S(1)}, u32[]{:S(2)}, u32[]{:S(2)}) %collective-permute-start.36) | collective-permute-done | bytes 131104 | tf_op jit(solution)/shard_map/ppermute | solution.py:127
  185.4 2.9 %collective-permute-done.43 = bf16[256,256]{1,0:T(8,128)(2,1)S(1)} collective-permute-done((bf16[256,256]{1,0:T(8,128)(2,1)S(1)}, bf16[256,256]{1,0:T(8,128)(2,1)S(1)}, u32[]{:S(2)}, u32[]{:S(2)}) %collective-permute-start.43) | collective-permute-done | bytes 131104 | tf_op jit(solution)/shard_map/ppermute | solution.py:127
  189.0 7.9 %collective-permute-done.45 = bf16[384,512]{1,0:T(8,128)(2,1)S(1)} collective-permute-done((bf16[384,512]{1,0:T(8,128)(2,1)S(1)}, bf16[384,512]{1,0:T(8,128)(2,1)S(1)}, u32[]{:S(2)}, u32[]{:S(2)}) %collective-permute-start.45) | collective-permute-done | bytes 393248 | tf_op jit(solution)/shard_map/ppermute | solution.py:133
  196.9 6.2 %collective-permute-done.46 = bf16[384,512]{1,0:T(8,128)(2,1)S(1)} collective-permute-done((bf16[384,512]{1,0:T(8,128)(2,1)S(1)}, bf16[384,512]{1,0:T(8,128)(2,1)S(1)}, u32[]{:S(2)}, u32[]{:S(2)}) %collective-permute-start.46) | collective-permute-done | bytes 393248 | tf_op jit(solution)/shard_map/ppermute | solution.py:133
  204.8 1.8 collective-permute-start.48
  209.7 3.5 %collective-permute-done.49.refs_2_ = bf16[384,128]{1,0:T(8,128)(2,1)S(1)} collective-permute-done((bf16[384,128]{1,0:T(8,128)(2,1)S(1)}, bf16[384,128]{1,0:T(8,128)(2,1)S(1)}, u32[]{:S(2)}, u32[]{:S(2)}) %collective-permute-start.49) | collective-permute-done | bytes 98336 | tf_op jit(solution)/shard_map/ppermute | solution.py:127
  213.1 2.5 %shard_map.87 = f32[128,1536]{1,0:T(8,128)} custom-call(s32[6]{0:T(128)S(1)} %copy-done.8, f32[384,128]{1,0:T(8,128)S(1)} %constant_dynamic-slice_fusion.refs_0_, bf16[384,128]{1,0:T(8,128)(2,1)S(1)} %collective-permute-done.48.refs_1_, bf16[384,128]{1,0:T(8,128)(2,1)S(1)} %collective-permute-done.49.refs_2_, ...), custom_call_target="tpu_custom_call" | custom-call | flops 1572864 | bytes 1572864 | tf_op jit(solution)/shard_map/pallas_call | solution.py:95
  215.7 1.9 shard_map.86
  (154 shorter events, 65.2 us)
Async XLA Ops:
  4.3 14.2 %collective-permute-start.1 = (bf16[128,1152]{1,0:T(8,128)(2,1)}, bf16[128,1152]{1,0:T(8,128)(2,1)S(1)}, u32[]{:S(2)}, u32[]{:S(2)}) collective-permute-start(bf16[128,1152]{1,0:T(8,128)(2,1)} %get-tuple-element.16), channel_id=1, source_target_pairs={{0,4},{2,6},{4,0},{6,2},{8,12},{10,14},{12,8},{14,10},{16,20},{18,... | collective-permute-start | bytes 884744 | tf_op jit(solution)/shard_map/ppermute | solution.py:127
  5.8 14.2 %collective-permute-start.2 = (bf16[128,1152]{1,0:T(8,128)(2,1)}, bf16[128,1152]{1,0:T(8,128)(2,1)S(1)}, u32[]{:S(2)}, u32[]{:S(2)}) collective-permute-start(bf16[128,1152]{1,0:T(8,128)(2,1)} %get-tuple-element.17), channel_id=1, source_target_pairs={{0,6},{2,4},{4,2},{6,0},{8,14},{10,12},{12,10},{14,8},{16,22},{18,... | collective-permute-start | bytes 884744 | tf_op jit(solution)/shard_map/ppermute | solution.py:127
  22.0 36.3 %collective-permute-start.9 = (bf16[384,768]{1,0:T(8,128)(2,1)}, bf16[384,768]{1,0:T(8,128)(2,1)}, u32[]{:S(2)}, u32[]{:S(2)}) collective-permute-start(bf16[384,768]{1,0:T(8,128)(2,1)} %get-tuple-element.20.refs_1_), channel_id=1, source_target_pairs={{0,8},{2,10},{4,12},{6,14},{8,24},{10,26},{12,28},{14,30},{16,0},{... | collective-permute-start | bytes 1769480 | tf_op jit(solution)/shard_map/ppermute | solution.py:130
  25.6 43.9 %collective-permute-start.12 = (bf16[256,2048]{1,0:T(8,128)(2,1)}, bf16[256,2048]{1,0:T(8,128)(2,1)}, u32[]{:S(2)}, u32[]{:S(2)}) collective-permute-start(bf16[256,2048]{1,0:T(8,128)(2,1)} %constant_dynamic-slice_fusion.2), channel_id=1, source_target_pairs={{0,2},{2,0},{4,6},{6,4},{8,10},{10,8},{12,14},{14,12},{16,18},{18,... | collective-permute-start | bytes 3145736 | tf_op jit(solution)/shard_map/ppermute | solution.py:127
  26.4 45.1 %collective-permute-start.17 = (bf16[256,2048]{1,0:T(8,128)(2,1)}, bf16[256,2048]{1,0:T(8,128)(2,1)S(1)}, u32[]{:S(2)}, u32[]{:S(2)}) collective-permute-start(bf16[256,2048]{1,0:T(8,128)(2,1)} %constant_dynamic-slice_fusion.2), channel_id=1, source_target_pairs={{0,4},{2,6},{4,0},{6,2},{8,12},{10,14},{12,8},{14,10},{16,20},{18,... | collective-permute-start | bytes 3145736 | tf_op jit(solution)/shard_map/ppermute | solution.py:127
  28.0 16.8 %collective-permute-start.3 = (bf16[128,1152]{1,0:T(8,128)(2,1)S(1)}, bf16[128,1152]{1,0:T(8,128)(2,1)}, u32[]{:S(2)}, u32[]{:S(2)}) collective-permute-start(bf16[128,1152]{1,0:T(8,128)(2,1)S(1)} %copy-done.4), channel_id=1, source_target_pairs={{0,8},{2,10},{4,12},{6,14},{8,24},{10,26},{12,28},{14,30},{16,0},{... | collective-permute-start | bytes 884744 | tf_op jit(solution)/shard_map/ppermute | solution.py:130
  28.4 22.7 %collective-permute-start.4 = (bf16[384,384]{1,0:T(8,128)(2,1)S(1)}, bf16[384,384]{1,0:T(8,128)(2,1)}, u32[]{:S(2)}, u32[]{:S(2)}) collective-permute-start(bf16[384,384]{1,0:T(8,128)(2,1)S(1)} %get-tuple-element.18.refs_1_), channel_id=1, source_target_pairs={{0,8},{2,10},{4,12},{6,14},{8,24},{10,26},{12,28},{14,30},{16,0},{... | collective-permute-start | bytes 884744 | tf_op jit(solution)/shard_map/ppermute | solution.py:130
  44.8 13.6 %collective-permute-start.5 = (bf16[128,1152]{1,0:T(8,128)(2,1)}, bf16[128,1152]{1,0:T(8,128)(2,1)}, u32[]{:S(2)}, u32[]{:S(2)}) collective-permute-start(bf16[128,1152]{1,0:T(8,128)(2,1)} %collective-permute-done.3.refs_2_), channel_id=1, source_target_pairs={{0,8},{2,10},{4,12},{6,14},{8,24},{10,26},{12,28},{14,30},{16,0},{... | collective-permute-start | bytes 884744 | tf_op jit(solution)/shard_map/ppermute | solution.py:130
  51.1 12.7 %collective-permute-start.6 = (bf16[384,384]{1,0:T(8,128)(2,1)}, bf16[384,384]{1,0:T(8,128)(2,1)}, u32[]{:S(2)}, u32[]{:S(2)}) collective-permute-start(bf16[384,384]{1,0:T(8,128)(2,1)} %collective-permute-done.4.refs_3_), channel_id=1, source_target_pairs={{0,8},{2,10},{4,12},{6,14},{8,24},{10,26},{12,28},{14,30},{16,0},{... | collective-permute-start | bytes 884744 | tf_op jit(solution)/shard_map/ppermute | solution.py:130
  58.3 30.3 %collective-permute-start.10 = (bf16[384,768]{1,0:T(8,128)(2,1)}, bf16[384,768]{1,0:T(8,128)(2,1)S(1)}, u32[]{:S(2)}, u32[]{:S(2)}) collective-permute-start(bf16[384,768]{1,0:T(8,128)(2,1)} %collective-permute-done.9.refs_3_), channel_id=1, source_target_pairs={{0,8},{2,10},{4,12},{6,14},{8,24},{10,26},{12,28},{14,30},{16,0},{... | collective-permute-start | bytes 1769480 | tf_op jit(solution)/shard_map/ppermute | solution.py:130
  58.4 24.4 %collective-permute-start.7 = (bf16[128,1152]{1,0:T(8,128)(2,1)}, bf16[128,1152]{1,0:T(8,128)(2,1)S(1)}, u32[]{:S(2)}, u32[]{:S(2)}) collective-permute-start(bf16[128,1152]{1,0:T(8,128)(2,1)} %collective-permute-done.5.refs_4_), channel_id=1, source_target_pairs={{0,8},{2,10},{4,12},{6,14},{8,24},{10,26},{12,28},{14,30},{16,0},{... | collective-permute-start | bytes 884744 | tf_op jit(solution)/shard_map/ppermute | solution.py:130
  63.9 23.3 %collective-permute-start.8 = (bf16[384,384]{1,0:T(8,128)(2,1)}, bf16[384,384]{1,0:T(8,128)(2,1)S(1)}, u32[]{:S(2)}, u32[]{:S(2)}) collective-permute-start(bf16[384,384]{1,0:T(8,128)(2,1)} %collective-permute-done.6.refs_5_), channel_id=1, source_target_pairs={{0,8},{2,10},{4,12},{6,14},{8,24},{10,26},{12,28},{14,30},{16,0},{... | collective-permute-start | bytes 884744 | tf_op jit(solution)/shard_map/ppermute | solution.py:130
  69.6 39.0 %collective-permute-start.14 = (bf16[512,768]{1,0:T(8,128)(2,1)S(1)}, bf16[512,768]{1,0:T(8,128)(2,1)S(1)}, u32[]{:S(2)}, u32[]{:S(2)}) collective-permute-start(bf16[512,768]{1,0:T(8,128)(2,1)S(1)} %get-tuple-element.21), channel_id=1, source_target_pairs={{0,2},{2,0},{4,6},{6,4},{8,10},{10,8},{12,14},{14,12},{16,18},{18,... | collective-permute-start | bytes 2359304 | tf_op jit(solution)/shard_map/ppermute | solution.py:127
  71.6 26.3 %collective-permute-start.21 = (bf16[128,2048]{1,0:T(8,128)(2,1)S(1)}, bf16[128,2048]{1,0:T(8,128)(2,1)S(1)}, u32[]{:S(2)}, u32[]{:S(2)}) collective-permute-start(bf16[128,2048]{1,0:T(8,128)(2,1)S(1)} %slice.189), channel_id=1, source_target_pairs={{0,4},{2,6},{4,0},{6,2},{8,12},{10,14},{12,8},{14,10},{16,20},{18,... | collective-permute-start | bytes 1572872 | tf_op jit(solution)/shard_map/ppermute | solution.py:127
  82.8 15.6 %collective-permute-start.22 = (bf16[128,2048]{1,0:T(8,128)(2,1)S(1)}, bf16[128,2048]{1,0:T(8,128)(2,1)S(1)}, u32[]{:S(2)}, u32[]{:S(2)}) collective-permute-start(bf16[128,2048]{1,0:T(8,128)(2,1)S(1)} %slice.190), channel_id=1, source_target_pairs={{0,2},{2,0},{4,6},{6,4},{8,10},{10,8},{12,14},{14,12},{16,18},{18,... | collective-permute-start | bytes 1572872 | tf_op jit(solution)/shard_map/ppermute | solution.py:127
  87.2 19.4 %collective-permute-start.13 = (bf16[256,2048]{1,0:T(8,128)(2,1)}, bf16[256,2048]{1,0:T(8,128)(2,1)S(1)}, u32[]{:S(2)}, u32[]{:S(2)}) collective-permute-start(bf16[256,2048]{1,0:T(8,128)(2,1)} %collective-permute-done.12.refs_0_), channel_id=1, source_target_pairs={{0,1},{1,0},{2,3},{3,2},{4,5},{5,4},{6,7},{7,6},{8,9},{9,8},{10,11... | collective-permute-start | bytes 3145736 | tf_op jit(solution)/shard_map/ppermute | solution.py:136
  88.6 16.8 %collective-permute-start.33 = (bf16[384,768]{1,0:T(8,128)(2,1)S(1)}, bf16[384,768]{1,0:T(8,128)(2,1)S(1)}, u32[]{:S(2)}, u32[]{:S(2)}) collective-permute-start(bf16[384,768]{1,0:T(8,128)(2,1)S(1)} %collective-permute-done.10.refs_5_), channel_id=1, source_target_pairs={{0,8},{2,10},{4,12},{6,14},{8,24},{10,26},{12,28},{14,30},{16,0},{... | collective-permute-start | bytes 1769480 | tf_op jit(solution)/shard_map/ppermute | solution.py:130
  97.9 20.7 %collective-permute-start.25 = (bf16[512,768]{1,0:T(8,128)(2,1)S(1)}, bf16[512,768]{1,0:T(8,128)(2,1)S(1)}, u32[]{:S(2)}, u32[]{:S(2)}) collective-permute-start(bf16[512,768]{1,0:T(8,128)(2,1)S(1)} %get-tuple-element.23), channel_id=1, source_target_pairs={{0,6},{2,4},{4,2},{6,0},{8,14},{10,12},{12,10},{14,8},{16,22},{18,... | collective-permute-start | bytes 2359304 | tf_op jit(solution)/shard_map/ppermute | solution.py:127
  106.6 28.8 %collective-permute-start.19 = (bf16[512,768]{1,0:T(8,128)(2,1)S(1)}, bf16[512,768]{1,0:T(8,128)(2,1)S(1)}, u32[]{:S(2)}, u32[]{:S(2)}) collective-permute-start(bf16[512,768]{1,0:T(8,128)(2,1)S(1)} %get-tuple-element.22), channel_id=1, source_target_pairs={{0,4},{2,6},{4,0},{6,2},{8,12},{10,14},{12,8},{14,10},{16,20},{18,... | collective-permute-start | bytes 2359304 | tf_op jit(solution)/shard_map/ppermute | solution.py:127
  108.6 12.1 %collective-permute-start.18 = (bf16[256,2048]{1,0:T(8,128)(2,1)S(1)}, bf16[256,2048]{1,0:T(8,128)(2,1)S(1)}, u32[]{:S(2)}, u32[]{:S(2)}) collective-permute-start(bf16[256,2048]{1,0:T(8,128)(2,1)S(1)} %collective-permute-done.17.refs_0_), channel_id=1, source_target_pairs={{0,1},{1,0},{2,3},{3,2},{4,5},{5,4},{6,7},{7,6},{8,9},{9,8},{10,11... | collective-permute-start | bytes 3145736 | tf_op jit(solution)/shard_map/ppermute | solution.py:136
  110.4 33.4 %collective-permute-start.11 = (bf16[256,1536]{1,0:T(8,128)(2,1)S(1)}, bf16[256,1536]{1,0:T(8,128)(2,1)S(1)}, u32[]{:S(2)}, u32[]{:S(2)}) collective-permute-start(bf16[256,1536]{1,0:T(8,128)(2,1)S(1)} %slice.177), channel_id=1, source_target_pairs={{0,1},{1,0},{2,3},{3,2},{4,5},{5,4},{6,7},{7,6},{8,9},{9,8},{10,11... | collective-permute-start | bytes 2359304 | tf_op jit(solution)/shard_map/ppermute | solution.py:136
  110.7 33.8 %collective-permute-start.34 = (bf16[256,512]{1,0:T(8,128)(2,1)S(1)}, bf16[256,512]{1,0:T(8,128)(2,1)S(1)}, u32[]{:S(2)}, u32[]{:S(2)}) collective-permute-start(bf16[256,512]{1,0:T(8,128)(2,1)S(1)} %slice.201), channel_id=1, source_target_pairs={{0,1},{1,0},{2,3},{3,2},{4,5},{5,4},{6,7},{7,6},{8,9},{9,8},{10,11... | collective-permute-start | bytes 786440 | tf_op jit(solution)/shard_map/ppermute | solution.py:136
  145.4 23.9 %collective-permute-start.42 = (bf16[256,256]{1,0:T(8,128)(2,1)S(1)}, bf16[256,256]{1,0:T(8,128)(2,1)S(1)}, u32[]{:S(2)}, u32[]{:S(2)}) collective-permute-start(bf16[256,256]{1,0:T(8,128)(2,1)S(1)} %get-tuple-element.45), channel_id=1, source_target_pairs={{0,4},{2,6},{4,0},{6,2},{8,12},{10,14},{12,8},{14,10},{16,20},{18,... | collective-permute-start | bytes 393224 | tf_op jit(solution)/shard_map/ppermute | solution.py:127
  146.1 24.4 %collective-permute-start.39 = (bf16[256,256]{1,0:T(8,128)(2,1)S(1)}, bf16[256,256]{1,0:T(8,128)(2,1)S(1)}, u32[]{:S(2)}, u32[]{:S(2)}) collective-permute-start(bf16[256,256]{1,0:T(8,128)(2,1)S(1)} %get-tuple-element.44), channel_id=1, source_target_pairs={{0,2},{2,0},{4,6},{6,4},{8,10},{10,8},{12,14},{14,12},{16,18},{18,... | collective-permute-start | bytes 393224 | tf_op jit(solution)/shard_map/ppermute | solution.py:127
  148.9 21.7 %collective-permute-start.16 = (bf16[256,768]{1,0:T(8,128)(2,1)S(1)}, bf16[256,768]{1,0:T(8,128)(2,1)S(1)}, u32[]{:S(2)}, u32[]{:S(2)}) collective-permute-start(bf16[256,768]{1,0:T(8,128)(2,1)S(1)} %slice.305), channel_id=1, source_target_pairs={{0,2},{2,0},{4,6},{6,4},{8,10},{10,8},{12,14},{14,12},{16,18},{18,... | collective-permute-start | bytes 1179656 | tf_op jit(solution)/shard_map/ppermute | solution.py:127
  150.4 17.8 %collective-permute-start.27 = (bf16[256,768]{1,0:T(8,128)(2,1)S(1)}, bf16[256,768]{1,0:T(8,128)(2,1)S(1)}, u32[]{:S(2)}, u32[]{:S(2)}) collective-permute-start(bf16[256,768]{1,0:T(8,128)(2,1)S(1)} %get-tuple-element.40), channel_id=1, source_target_pairs={{0,2},{2,0},{4,6},{6,4},{8,10},{10,8},{12,14},{14,12},{16,18},{18,... | collective-permute-start | bytes 1179656 | tf_op jit(solution)/shard_map/ppermute | solution.py:127
  159.3 12.5 %collective-permute-start.29 = (bf16[256,768]{1,0:T(8,128)(2,1)S(1)}, bf16[256,768]{1,0:T(8,128)(2,1)S(1)}, u32[]{:S(2)}, u32[]{:S(2)}) collective-permute-start(bf16[256,768]{1,0:T(8,128)(2,1)S(1)} %slice.304), channel_id=1, source_target_pairs={{0,4},{2,6},{4,0},{6,2},{8,12},{10,14},{12,8},{14,10},{16,20},{18,... | collective-permute-start | bytes 1179656 | tf_op jit(solution)/shard_map/ppermute | solution.py:127
  170.5 26.4 %collective-permute-start.45 = (bf16[384,512]{1,0:T(8,128)(2,1)S(1)}, bf16[384,512]{1,0:T(8,128)(2,1)S(1)}, u32[]{:S(2)}, u32[]{:S(2)}) collective-permute-start(bf16[384,512]{1,0:T(8,128)(2,1)S(1)} %get-tuple-element.24), channel_id=1, source_target_pairs={{0,8},{2,10},{4,12},{6,14},{8,16},{10,18},{12,20},{14,22},{16,24},... | collective-permute-start | bytes 1179656 | tf_op jit(solution)/shard_map/ppermute | solution.py:133
  170.6 32.5 %collective-permute-start.46 = (bf16[384,512]{1,0:T(8,128)(2,1)S(1)}, bf16[384,512]{1,0:T(8,128)(2,1)S(1)}, u32[]{:S(2)}, u32[]{:S(2)}) collective-permute-start(bf16[384,512]{1,0:T(8,128)(2,1)S(1)} %get-tuple-element.26), channel_id=1, source_target_pairs={{0,16},{2,18},{4,20},{6,22},{8,24},{10,26},{12,28},{14,30},{16,0},... | collective-permute-start | bytes 1179656 | tf_op jit(solution)/shard_map/ppermute | solution.py:133
  171.8 32.7 %collective-permute-start.47 = (bf16[384,512]{1,0:T(8,128)(2,1)S(1)}, bf16[384,512]{1,0:T(8,128)(2,1)S(1)}, u32[]{:S(2)}, u32[]{:S(2)}) collective-permute-start(bf16[384,512]{1,0:T(8,128)(2,1)S(1)} %get-tuple-element.25), channel_id=1, source_target_pairs={{0,24},{2,26},{4,28},{6,30},{8,0},{10,2},{12,4},{14,6},{16,8},{18,... | collective-permute-start | bytes 1179656 | tf_op jit(solution)/shard_map/ppermute | solution.py:133
  188.3 27.4 %collective-permute-start.32 = (bf16[256,1536]{1,0:T(8,128)(2,1)S(1)}, bf16[256,1536]{1,0:T(8,128)(2,1)S(1)}, u32[]{:S(2)}, u32[]{:S(2)}) collective-permute-start(bf16[256,1536]{1,0:T(8,128)(2,1)S(1)} %pad_maximum_fusion.7.refs_0_), channel_id=1, source_target_pairs={{0,1},{1,0},{2,3},{3,2},{4,5},{5,4},{6,7},{7,6},{8,9},{9,8},{10,11... | collective-permute-start | bytes 2359304 | tf_op jit(solution)/shard_map/ppermute | solution.py:136
  188.9 26.8 %collective-permute-start.44 = (bf16[256,512]{1,0:T(8,128)(2,1)S(1)}, bf16[256,512]{1,0:T(8,128)(2,1)S(1)}, u32[]{:S(2)}, u32[]{:S(2)}) collective-permute-start(bf16[256,512]{1,0:T(8,128)(2,1)S(1)} %pad_maximum_fusion.16.refs_2_), channel_id=1, source_target_pairs={{0,1},{1,0},{2,3},{3,2},{4,5},{5,4},{6,7},{7,6},{8,9},{9,8},{10,11... | collective-permute-start | bytes 786440 | tf_op jit(solution)/shard_map/ppermute | solution.py:136
  (28 other events, 278.1 us)

commit v2 on v1

--- a/solution.py
+++ b/solution.py
@@ -12,9 +12,10 @@
 B = 4
 
 
-def pack_weights_kernel(fb, at_ref, d_ref, g_ref, u_ref, *outs):
+def pack_weights_kernel(fb, d_ref, g_ref, u_ref, *outs):
+    q = lax.rem(lax.axis_index("fs"), B)
     for k in range(B):
-        at = pl.ds(pl.multiple_of((at_ref[0] ^ k) * fb, 128), fb)
+        at = pl.ds(pl.multiple_of((q ^ k) * fb, 128), fb)
         outs[k][:, :fb] = d_ref[:, at]
         outs[k][:, fb : 2 * fb] = g_ref[:, at]
         outs[k][:, 2 * fb :] = u_ref[:, at]
@@ -105,16 +106,16 @@
 
 def packed(kernel, at, arrays, shapes, dtype=BF16, limit=True):
     whole = pl.BlockSpec()
-    inside = pl.BlockSpec(memory_space=pltpu.VMEM) if limit == 2 else whole
+    first = [] if at is None else [at]
     moved = 2 * sum(v.size for v in arrays) + 2 * sum(math.prod(x) for x in shapes)
     return pl.pallas_call(
         kernel,
-        in_specs=[pl.BlockSpec(memory_space=pltpu.SMEM)] + [inside] * len(arrays),
+        in_specs=[pl.BlockSpec(memory_space=pltpu.SMEM)] * len(first) + [whole] * len(arrays),
         out_specs=[whole] * len(shapes),
         out_shape=[jax.ShapeDtypeStruct(s, dtype) for s in shapes],
         compiler_params=pltpu.CompilerParams(vmem_limit_bytes=moved + (3 << 20) if limit else None),
         cost_estimate=pl.CostEstimate(flops=moved, bytes_accessed=moved, transcendentals=0),
-    )(at, *arrays)
+    )(*first, *arrays)
 
 
 def make_local(n, tp):
@@ -175,17 +176,17 @@
         if tiled:
             packs = packed(
                 functools.partial(pack_weights_kernel, fb),
-                at,
+                None,
                 (wd, wg, wu),
                 [(wrows, 3 * fb)] * B,
-                limit=0,
+                limit=False,
             )
             tok = packed(
                 functools.partial(pack_tokens_kernel, fb, half, tp),
                 at,
                 (g, u),
                 [(tokens, 2 * fb)] * B,
-                limit=1,
+                limit=False,
             )
         else:
             packs = [jnp.concatenate([cols(v, q ^ k) for v in (wd, wg, wu)], 1) for k in range(B)]

time: 218 us -> 217 us (level)
  local copies, waits for them, and re-layouts: 7.07 us -> 3.64 us
  Pallas kernels: 15.3 us -> 18.5 us
    pallas_call x9, Pallas kernels: 10.9 us -> 14.1 us  [packed(): pl.pallas_call(kernel, in_specs=[pl.BlockSpec(memory_space=pltpu.SMEM)] *...]
    unnamed x18 -> x22, local copies, waits for them, and re-layouts: 3.44 us -> 0.53 us
  transfers between devices with their start and end apart: 51 -> 51, of which waited for: 24 -> 23; matrix products, arithmetic and copies ran while one was open for 12% -> 12% of each run, Pallas kernels for 4% -> 6%
where the time goes in v2:
time: 217 us
  waiting for transfers between devices  120 us (55%)
  starting transfers between devices  49.9 us (23%)
  matrix products  21.2 us (10%)
  Pallas kernels  18.5 us (9%)
  local copies, waits for them, and re-layouts  3.64 us (2%)
    ppermute x25, waiting for transfers between devices, xperm(): lax.ppermute(v, 'fs', [(j, j // B * B + (j % B ^ k)) for j in range(n)])  62 us
    ppermute x9, waiting for transfers between devices, zring(): lax.ppermute(v, 'fs', [(j, after[j // B] * B + j % B) for j in range(n)])  41.8 us
    ppermute x25, starting transfers between devices, xperm(): lax.ppermute(v, 'fs', [(j, j // B * B + (j % B ^ k)) for j in range(n)])  24.9 us
    ppermute x9, starting transfers between devices, zring(): lax.ppermute(v, 'fs', [(j, after[j // B] * B + j % B) for j in range(n)])  19.6 us
    ppermute x3, waiting for transfers between devices, zshift(): lax.ppermute(v, 'fs', [(j, (j // B + s) % a * B + j % B) for j in range(n)])  15.5 us
    pallas_call x9, Pallas kernels, packed(): pl.pallas_call(kernel, in_specs=[pl.BlockSpec(memory_space=pltpu.SMEM)] *...  14.1 us
    dot_general x8, matrix products, local(): lax.dot_general(dgus[k], wgu, (((1,), (1,)), ((), ())), preferred_element...  8.11 us
    dot_general x4, matrix products, local(): dh = jnp.dot(cots[k], wd_full, preferred_element_type=F32)  7.04 us
  transfers between devices with their start and end apart: 51, of which 23 were waited for; matrix products, arithmetic and copies ran while one was open for 12% of the time, Pallas kernels for 6%

profile of v2, /device:TPU:10, one launch (start us, length us, event | category | flops | bytes accessed | tf_op | source)
XLA Modules:
  0.0 216.6 jit_solution(11187299628699893063)
XLA Ops:
  0.6 2.5 %shard_map.77 = (bf16[128,1152]{1,0:T(8,128)(2,1)}, bf16[128,1152]{1,0:T(8,128)(2,1)}, bf16[128,1152]{1,0:T(8,128)(2,1)}, bf16[128,1152]{1,0:T(8,128)(2,1)}) custom-call(bf16[128,1536]{1,0:T(8,128)(2,1)} %d_ref.1, bf16[128,1536]{1,0:T(8,128)(2,1)} %g_ref.2, bf16[128,1536]{1,0:T(8,128)(2,1)} %u_ref.2), custom_call_target="tpu_custom_call" | custom-call | flops 2359296 | bytes 2359296 | tf_op jit(solution)/shard_map/pallas_call | solution.py:111
  6.7 6.5 %collective-permute-done.refs_0_ = bf16[128,1152]{1,0:T(8,128)(2,1)S(1)} collective-permute-done((bf16[128,1152]{1,0:T(8,128)(2,1)}, bf16[128,1152]{1,0:T(8,128)(2,1)S(1)}, u32[]{:S(2)}, u32[]{:S(2)}) %collective-permute-start) | collective-permute-done | bytes 294944 | tf_op jit(solution)/shard_map/ppermute | solution.py:128
  13.2 4.6 %collective-permute-done.1.refs_1_ = bf16[128,1152]{1,0:T(8,128)(2,1)S(1)} collective-permute-done((bf16[128,1152]{1,0:T(8,128)(2,1)}, bf16[128,1152]{1,0:T(8,128)(2,1)S(1)}, u32[]{:S(2)}, u32[]{:S(2)}) %collective-permute-start.1) | collective-permute-done | bytes 294944 | tf_op jit(solution)/shard_map/ppermute | solution.py:128
  20.8 2.6 %collective-permute-start.9 = (bf16[384,768]{1,0:T(8,128)(2,1)}, bf16[384,768]{1,0:T(8,128)(2,1)}, u32[]{:S(2)}, u32[]{:S(2)}) collective-permute-start(bf16[384,768]{1,0:T(8,128)(2,1)} %get-tuple-element.20.refs_1_), channel_id=1, source_target_pairs={{0,8},{2,10},{4,12},{6,14},{8,24},{10,26},{12,28},{14,30},{16,0},{... | collective-permute-start | bytes 1769480 | tf_op jit(solution)/shard_map/ppermute | solution.py:131
  27.6 16.1 %collective-permute-done.3.refs_2_ = bf16[128,1152]{1,0:T(8,128)(2,1)} collective-permute-done((bf16[128,1152]{1,0:T(8,128)(2,1)S(1)}, bf16[128,1152]{1,0:T(8,128)(2,1)}, u32[]{:S(2)}, u32[]{:S(2)}) %collective-permute-start.3) | collective-permute-done | bytes 294944 | tf_op jit(solution)/shard_map/ppermute | solution.py:131
  43.7 3.5 %collective-permute-start.5 = (bf16[128,1152]{1,0:T(8,128)(2,1)}, bf16[128,1152]{1,0:T(8,128)(2,1)}, u32[]{:S(2)}, u32[]{:S(2)}) collective-permute-start(bf16[128,1152]{1,0:T(8,128)(2,1)} %collective-permute-done.3.refs_2_), channel_id=1, source_target_pairs={{0,8},{2,10},{4,12},{6,14},{8,24},{10,26},{12,28},{14,30},{16,0},{... | collective-permute-start | bytes 884744 | tf_op jit(solution)/shard_map/ppermute | solution.py:131
  47.2 2.8 %collective-permute-done.4.refs_3_ = bf16[384,384]{1,0:T(8,128)(2,1)} collective-permute-done((bf16[384,384]{1,0:T(8,128)(2,1)S(1)}, bf16[384,384]{1,0:T(8,128)(2,1)}, u32[]{:S(2)}, u32[]{:S(2)}) %collective-permute-start.4) | collective-permute-done | bytes 294944 | tf_op jit(solution)/shard_map/ppermute | solution.py:131
  50.0 3.5 %collective-permute-start.6 = (bf16[384,384]{1,0:T(8,128)(2,1)}, bf16[384,384]{1,0:T(8,128)(2,1)}, u32[]{:S(2)}, u32[]{:S(2)}) collective-permute-start(bf16[384,384]{1,0:T(8,128)(2,1)} %collective-permute-done.4.refs_3_), channel_id=1, source_target_pairs={{0,8},{2,10},{4,12},{6,14},{8,24},{10,26},{12,28},{14,30},{16,0},{... | collective-permute-start | bytes 884744 | tf_op jit(solution)/shard_map/ppermute | solution.py:131
  53.5 3.8 %shard_map.80 = (bf16[512,768]{1,0:T(8,128)(2,1)}, bf16[512,768]{1,0:T(8,128)(2,1)}, bf16[512,768]{1,0:T(8,128)(2,1)}, bf16[512,768]{1,0:T(8,128)(2,1)}) custom-call(s32[6]{0:T(128)} %copy-done.5, bf16[512,1536]{1,0:T(8,128)(2,1)} %g_ref.3, bf16[512,1536]{1,0:T(8,128)(2,1)} %u_ref.3), custom_call_target="tpu_custom_call" | custom-call | flops 6291456 | bytes 6291456 | tf_op jit(solution)/shard_map/pallas_call | solution.py:111
  57.5 2.3 %collective-permute-start.7 = (bf16[128,1152]{1,0:T(8,128)(2,1)}, bf16[128,1152]{1,0:T(8,128)(2,1)S(1)}, u32[]{:S(2)}, u32[]{:S(2)}) collective-permute-start(bf16[128,1152]{1,0:T(8,128)(2,1)} %collective-permute-done.5.refs_4_), channel_id=1, source_target_pairs={{0,8},{2,10},{4,12},{6,14},{8,24},{10,26},{12,28},{14,30},{16,0},{... | collective-permute-start | bytes 884744 | tf_op jit(solution)/shard_map/ppermute | solution.py:131
  59.8 2.9 %collective-permute-done.6.refs_5_ = bf16[384,384]{1,0:T(8,128)(2,1)} collective-permute-done((bf16[384,384]{1,0:T(8,128)(2,1)}, bf16[384,384]{1,0:T(8,128)(2,1)}, u32[]{:S(2)}, u32[]{:S(2)}) %collective-permute-start.6) | collective-permute-done | bytes 294944 | tf_op jit(solution)/shard_map/ppermute | solution.py:131
  62.7 3.4 %collective-permute-start.8 = (bf16[384,384]{1,0:T(8,128)(2,1)}, bf16[384,384]{1,0:T(8,128)(2,1)S(1)}, u32[]{:S(2)}, u32[]{:S(2)}) collective-permute-start(bf16[384,384]{1,0:T(8,128)(2,1)} %collective-permute-done.6.refs_5_), channel_id=1, source_target_pairs={{0,8},{2,10},{4,12},{6,14},{8,24},{10,26},{12,28},{14,30},{16,0},{... | collective-permute-start | bytes 884744 | tf_op jit(solution)/shard_map/ppermute | solution.py:131
  66.1 2.4 %fusion = f32[384,2048]{1,0:T(8,128)S(1)} fusion(bf16[256,2048]{1,0:T(8,128)(2,1)S(1)} %constant_dynamic-slice_fusion.1, bf16[256,2048]{1,0:T(8,128)(2,1)} %constant_dynamic-slice_fusion.2, bf16[512,768]{1,0:T(8,128)(2,1)S(1)} %copy-done.10), kind=kOutput, calls=%fused_computation.26 | convolution fusion | flops 811073536 | bytes 6029312 | tf_op jit(solution)/shard_map/dot_general | solution.py:248
  72.2 9.5 %collective-permute-done.7.refs_6_.refs_0_ = bf16[128,1152]{1,0:T(8,128)(2,1)S(1)} collective-permute-done((bf16[128,1152]{1,0:T(8,128)(2,1)}, bf16[128,1152]{1,0:T(8,128)(2,1)S(1)}, u32[]{:S(2)}, u32[]{:S(2)}) %collective-permute-start.7) | collective-permute-done | bytes 294944 | tf_op jit(solution)/shard_map/ppermute | solution.py:131
  82.5 3.5 %collective-permute-done.8.refs_7_ = bf16[384,384]{1,0:T(8,128)(2,1)S(1)} collective-permute-done((bf16[384,384]{1,0:T(8,128)(2,1)}, bf16[384,384]{1,0:T(8,128)(2,1)S(1)}, u32[]{:S(2)}, u32[]{:S(2)}) %collective-permute-start.8) | collective-permute-done | bytes 294944 | tf_op jit(solution)/shard_map/ppermute | solution.py:131
  87.4 3.5 %collective-permute-start.33 = (bf16[384,768]{1,0:T(8,128)(2,1)S(1)}, bf16[384,768]{1,0:T(8,128)(2,1)S(1)}, u32[]{:S(2)}, u32[]{:S(2)}) collective-permute-start(bf16[384,768]{1,0:T(8,128)(2,1)S(1)} %collective-permute-done.10.refs_5_), channel_id=1, source_target_pairs={{0,8},{2,10},{4,12},{6,14},{8,24},{10,26},{12,28},{14,30},{16,0},{... | collective-permute-start | bytes 1769480 | tf_op jit(solution)/shard_map/ppermute | solution.py:131
  90.9 2.7 %fusion.4 = (bf16[512,384]{1,0:T(8,128)(2,1)S(1)}, bf16[512,384]{1,0:T(8,128)(2,1)S(1)}) fusion(bf16[512,768]{1,0:T(8,128)(2,1)S(1)} %copy-done.10, bf16[2048,384]{1,0:T(8,128)(2,1)S(1)} %shard_map.79, bf16[256,2048]{1,0:T(8,128)(2,1)S(1)} %constant_dynamic-slice_fusion.1, bf16[256,2048]{1,0:T(8,128)(2,1)} %constant_dynamic-slice_fusion.2), kind=kOutput, calls=%fused_computation.42 | convolution fusion | flops 812449792 | bytes 5242880 | tf_op jit(solution)/shard_map/dot_general | solution.py:244
  97.3 6.9 %collective-permute-done.33.refs_1_ = bf16[384,768]{1,0:T(8,128)(2,1)S(1)} collective-permute-done((bf16[384,768]{1,0:T(8,128)(2,1)S(1)}, bf16[384,768]{1,0:T(8,128)(2,1)S(1)}, u32[]{:S(2)}, u32[]{:S(2)}) %collective-permute-start.33) | collective-permute-done | bytes 589856 | tf_op jit(solution)/shard_map/ppermute | solution.py:131
  111.5 6.0 %collective-permute-done.25 = bf16[512,768]{1,0:T(8,128)(2,1)S(1)} collective-permute-done((bf16[512,768]{1,0:T(8,128)(2,1)S(1)}, bf16[512,768]{1,0:T(8,128)(2,1)S(1)}, u32[]{:S(2)}, u32[]{:S(2)}) %collective-permute-start.25) | collective-permute-done | bytes 786464 | tf_op jit(solution)/shard_map/ppermute | solution.py:128
  123.1 11.1 %collective-permute-done.19 = bf16[512,768]{1,0:T(8,128)(2,1)S(1)} collective-permute-done((bf16[512,768]{1,0:T(8,128)(2,1)S(1)}, bf16[512,768]{1,0:T(8,128)(2,1)S(1)}, u32[]{:S(2)}, u32[]{:S(2)}) %collective-permute-start.19) | collective-permute-done | bytes 786464 | tf_op jit(solution)/shard_map/ppermute | solution.py:128
  150.1 8.0 %collective-permute-done.30 = bf16[256,768]{1,0:T(8,128)(2,1)S(1)} collective-permute-done((bf16[256,768]{1,0:T(8,128)(2,1)S(1)}, bf16[256,768]{1,0:T(8,128)(2,1)S(1)}, u32[]{:S(2)}, u32[]{:S(2)}) %collective-permute-start.30) | collective-permute-done | bytes 393248 | tf_op jit(solution)/shard_map/ppermute | solution.py:128
  158.8 8.2 %collective-permute-done.27 = bf16[256,768]{1,0:T(8,128)(2,1)S(1)} collective-permute-done((bf16[256,768]{1,0:T(8,128)(2,1)S(1)}, bf16[256,768]{1,0:T(8,128)(2,1)S(1)}, u32[]{:S(2)}, u32[]{:S(2)}) %collective-permute-start.27) | collective-permute-done | bytes 393248 | tf_op jit(solution)/shard_map/ppermute | solution.py:128
  171.8 5.1 %collective-permute-done.31 = bf16[256,768]{1,0:T(8,128)(2,1)S(1)} collective-permute-done((bf16[256,768]{1,0:T(8,128)(2,1)S(1)}, bf16[256,768]{1,0:T(8,128)(2,1)S(1)}, u32[]{:S(2)}, u32[]{:S(2)}) %collective-permute-start.31) | collective-permute-done | bytes 393248 | tf_op jit(solution)/shard_map/ppermute | solution.py:128
  177.4 1.8 collective-permute-start.41
  179.4 2.7 %collective-permute-done.36 = bf16[256,256]{1,0:T(8,128)(2,1)S(1)} collective-permute-done((bf16[256,256]{1,0:T(8,128)(2,1)S(1)}, bf16[256,256]{1,0:T(8,128)(2,1)S(1)}, u32[]{:S(2)}, u32[]{:S(2)}) %collective-permute-start.36) | collective-permute-done | bytes 131104 | tf_op jit(solution)/shard_map/ppermute | solution.py:128
  184.2 2.9 %collective-permute-done.43 = bf16[256,256]{1,0:T(8,128)(2,1)S(1)} collective-permute-done((bf16[256,256]{1,0:T(8,128)(2,1)S(1)}, bf16[256,256]{1,0:T(8,128)(2,1)S(1)}, u32[]{:S(2)}, u32[]{:S(2)}) %collective-permute-start.43) | collective-permute-done | bytes 131104 | tf_op jit(solution)/shard_map/ppermute | solution.py:128
  187.8 7.9 %collective-permute-done.45 = bf16[384,512]{1,0:T(8,128)(2,1)S(1)} collective-permute-done((bf16[384,512]{1,0:T(8,128)(2,1)S(1)}, bf16[384,512]{1,0:T(8,128)(2,1)S(1)}, u32[]{:S(2)}, u32[]{:S(2)}) %collective-permute-start.45) | collective-permute-done | bytes 393248 | tf_op jit(solution)/shard_map/ppermute | solution.py:134
  195.7 6.2 %collective-permute-done.46 = bf16[384,512]{1,0:T(8,128)(2,1)S(1)} collective-permute-done((bf16[384,512]{1,0:T(8,128)(2,1)S(1)}, bf16[384,512]{1,0:T(8,128)(2,1)S(1)}, u32[]{:S(2)}, u32[]{:S(2)}) %collective-permute-start.46) | collective-permute-done | bytes 393248 | tf_op jit(solution)/shard_map/ppermute | solution.py:134
  203.6 1.8 collective-permute-start.48
  208.5 3.5 %collective-permute-done.49.refs_2_ = bf16[384,128]{1,0:T(8,128)(2,1)S(1)} collective-permute-done((bf16[384,128]{1,0:T(8,128)(2,1)S(1)}, bf16[384,128]{1,0:T(8,128)(2,1)S(1)}, u32[]{:S(2)}, u32[]{:S(2)}) %collective-permute-start.49) | collective-permute-done | bytes 98336 | tf_op jit(solution)/shard_map/ppermute | solution.py:128
  212.0 2.5 %shard_map.87 = f32[128,1536]{1,0:T(8,128)} custom-call(s32[6]{0:T(128)S(1)} %copy-done.6, f32[384,128]{1,0:T(8,128)S(1)} %constant_dynamic-slice_fusion.refs_0_, bf16[384,128]{1,0:T(8,128)(2,1)S(1)} %collective-permute-done.48.refs_1_, bf16[384,128]{1,0:T(8,128)(2,1)S(1)} %collective-permute-done.49.refs_2_, ...), custom_call_target="tpu_custom_call" | custom-call | flops 1572864 | bytes 1572864 | tf_op jit(solution)/shard_map/pallas_call | solution.py:96
  214.5 1.9 shard_map.86
  (158 shorter events, 62.3 us)
Async XLA Ops:
  3.7 14.2 %collective-permute-start.1 = (bf16[128,1152]{1,0:T(8,128)(2,1)}, bf16[128,1152]{1,0:T(8,128)(2,1)S(1)}, u32[]{:S(2)}, u32[]{:S(2)}) collective-permute-start(bf16[128,1152]{1,0:T(8,128)(2,1)} %get-tuple-element.16), channel_id=1, source_target_pairs={{0,4},{2,6},{4,0},{6,2},{8,12},{10,14},{12,8},{14,10},{16,20},{18,... | collective-permute-start | bytes 884744 | tf_op jit(solution)/shard_map/ppermute | solution.py:128
  5.2 14.2 %collective-permute-start.2 = (bf16[128,1152]{1,0:T(8,128)(2,1)}, bf16[128,1152]{1,0:T(8,128)(2,1)S(1)}, u32[]{:S(2)}, u32[]{:S(2)}) collective-permute-start(bf16[128,1152]{1,0:T(8,128)(2,1)} %get-tuple-element.17), channel_id=1, source_target_pairs={{0,6},{2,4},{4,2},{6,0},{8,14},{10,12},{12,10},{14,8},{16,22},{18,... | collective-permute-start | bytes 884744 | tf_op jit(solution)/shard_map/ppermute | solution.py:128
  20.8 36.5 %collective-permute-start.9 = (bf16[384,768]{1,0:T(8,128)(2,1)}, bf16[384,768]{1,0:T(8,128)(2,1)}, u32[]{:S(2)}, u32[]{:S(2)}) collective-permute-start(bf16[384,768]{1,0:T(8,128)(2,1)} %get-tuple-element.20.refs_1_), channel_id=1, source_target_pairs={{0,8},{2,10},{4,12},{6,14},{8,24},{10,26},{12,28},{14,30},{16,0},{... | collective-permute-start | bytes 1769480 | tf_op jit(solution)/shard_map/ppermute | solution.py:131
  24.5 44.0 %collective-permute-start.12 = (bf16[256,2048]{1,0:T(8,128)(2,1)}, bf16[256,2048]{1,0:T(8,128)(2,1)}, u32[]{:S(2)}, u32[]{:S(2)}) collective-permute-start(bf16[256,2048]{1,0:T(8,128)(2,1)} %constant_dynamic-slice_fusion.2), channel_id=1, source_target_pairs={{0,2},{2,0},{4,6},{6,4},{8,10},{10,8},{12,14},{14,12},{16,18},{18,... | collective-permute-start | bytes 3145736 | tf_op jit(solution)/shard_map/ppermute | solution.py:128
  25.3 45.2 %collective-permute-start.17 = (bf16[256,2048]{1,0:T(8,128)(2,1)}, bf16[256,2048]{1,0:T(8,128)(2,1)S(1)}, u32[]{:S(2)}, u32[]{:S(2)}) collective-permute-start(bf16[256,2048]{1,0:T(8,128)(2,1)} %constant_dynamic-slice_fusion.2), channel_id=1, source_target_pairs={{0,4},{2,6},{4,0},{6,2},{8,12},{10,14},{12,8},{14,10},{16,20},{18,... | collective-permute-start | bytes 3145736 | tf_op jit(solution)/shard_map/ppermute | solution.py:128
  26.8 16.8 %collective-permute-start.3 = (bf16[128,1152]{1,0:T(8,128)(2,1)S(1)}, bf16[128,1152]{1,0:T(8,128)(2,1)}, u32[]{:S(2)}, u32[]{:S(2)}) collective-permute-start(bf16[128,1152]{1,0:T(8,128)(2,1)S(1)} %copy-done.2), channel_id=1, source_target_pairs={{0,8},{2,10},{4,12},{6,14},{8,24},{10,26},{12,28},{14,30},{16,0},{... | collective-permute-start | bytes 884744 | tf_op jit(solution)/shard_map/ppermute | solution.py:131
  27.3 22.7 %collective-permute-start.4 = (bf16[384,384]{1,0:T(8,128)(2,1)S(1)}, bf16[384,384]{1,0:T(8,128)(2,1)}, u32[]{:S(2)}, u32[]{:S(2)}) collective-permute-start(bf16[384,384]{1,0:T(8,128)(2,1)S(1)} %get-tuple-element.18.refs_1_), channel_id=1, source_target_pairs={{0,8},{2,10},{4,12},{6,14},{8,24},{10,26},{12,28},{14,30},{16,0},{... | collective-permute-start | bytes 884744 | tf_op jit(solution)/shard_map/ppermute | solution.py:131
  43.7 13.8 %collective-permute-start.5 = (bf16[128,1152]{1,0:T(8,128)(2,1)}, bf16[128,1152]{1,0:T(8,128)(2,1)}, u32[]{:S(2)}, u32[]{:S(2)}) collective-permute-start(bf16[128,1152]{1,0:T(8,128)(2,1)} %collective-permute-done.3.refs_2_), channel_id=1, source_target_pairs={{0,8},{2,10},{4,12},{6,14},{8,24},{10,26},{12,28},{14,30},{16,0},{... | collective-permute-start | bytes 884744 | tf_op jit(solution)/shard_map/ppermute | solution.py:131
  50.0 12.7 %collective-permute-start.6 = (bf16[384,384]{1,0:T(8,128)(2,1)}, bf16[384,384]{1,0:T(8,128)(2,1)}, u32[]{:S(2)}, u32[]{:S(2)}) collective-permute-start(bf16[384,384]{1,0:T(8,128)(2,1)} %collective-permute-done.4.refs_3_), channel_id=1, source_target_pairs={{0,8},{2,10},{4,12},{6,14},{8,24},{10,26},{12,28},{14,30},{16,0},{... | collective-permute-start | bytes 884744 | tf_op jit(solution)/shard_map/ppermute | solution.py:131
  57.3 30.1 %collective-permute-start.10 = (bf16[384,768]{1,0:T(8,128)(2,1)}, bf16[384,768]{1,0:T(8,128)(2,1)S(1)}, u32[]{:S(2)}, u32[]{:S(2)}) collective-permute-start(bf16[384,768]{1,0:T(8,128)(2,1)} %collective-permute-done.9.refs_3_), channel_id=1, source_target_pairs={{0,8},{2,10},{4,12},{6,14},{8,24},{10,26},{12,28},{14,30},{16,0},{... | collective-permute-start | bytes 1769480 | tf_op jit(solution)/shard_map/ppermute | solution.py:131
  57.5 24.2 %collective-permute-start.7 = (bf16[128,1152]{1,0:T(8,128)(2,1)}, bf16[128,1152]{1,0:T(8,128)(2,1)S(1)}, u32[]{:S(2)}, u32[]{:S(2)}) collective-permute-start(bf16[128,1152]{1,0:T(8,128)(2,1)} %collective-permute-done.5.refs_4_), channel_id=1, source_target_pairs={{0,8},{2,10},{4,12},{6,14},{8,24},{10,26},{12,28},{14,30},{16,0},{... | collective-permute-start | bytes 884744 | tf_op jit(solution)/shard_map/ppermute | solution.py:131
  62.7 23.3 %collective-permute-start.8 = (bf16[384,384]{1,0:T(8,128)(2,1)}, bf16[384,384]{1,0:T(8,128)(2,1)S(1)}, u32[]{:S(2)}, u32[]{:S(2)}) collective-permute-start(bf16[384,384]{1,0:T(8,128)(2,1)} %collective-permute-done.6.refs_5_), channel_id=1, source_target_pairs={{0,8},{2,10},{4,12},{6,14},{8,24},{10,26},{12,28},{14,30},{16,0},{... | collective-permute-start | bytes 884744 | tf_op jit(solution)/shard_map/ppermute | solution.py:131
  68.6 39.3 %collective-permute-start.14 = (bf16[512,768]{1,0:T(8,128)(2,1)S(1)}, bf16[512,768]{1,0:T(8,128)(2,1)S(1)}, u32[]{:S(2)}, u32[]{:S(2)}) collective-permute-start(bf16[512,768]{1,0:T(8,128)(2,1)S(1)} %copy-done.9), channel_id=1, source_target_pairs={{0,2},{2,0},{4,6},{6,4},{8,10},{10,8},{12,14},{14,12},{16,18},{18,... | collective-permute-start | bytes 2359304 | tf_op jit(solution)/shard_map/ppermute | solution.py:128
  70.5 26.2 %collective-permute-start.21 = (bf16[128,2048]{1,0:T(8,128)(2,1)S(1)}, bf16[128,2048]{1,0:T(8,128)(2,1)S(1)}, u32[]{:S(2)}, u32[]{:S(2)}) collective-permute-start(bf16[128,2048]{1,0:T(8,128)(2,1)S(1)} %slice.189), channel_id=1, source_target_pairs={{0,4},{2,6},{4,0},{6,2},{8,12},{10,14},{12,8},{14,10},{16,20},{18,... | collective-permute-start | bytes 1572872 | tf_op jit(solution)/shard_map/ppermute | solution.py:128
  81.7 15.6 %collective-permute-start.22 = (bf16[128,2048]{1,0:T(8,128)(2,1)S(1)}, bf16[128,2048]{1,0:T(8,128)(2,1)S(1)}, u32[]{:S(2)}, u32[]{:S(2)}) collective-permute-start(bf16[128,2048]{1,0:T(8,128)(2,1)S(1)} %slice.190), channel_id=1, source_target_pairs={{0,2},{2,0},{4,6},{6,4},{8,10},{10,8},{12,14},{14,12},{16,18},{18,... | collective-permute-start | bytes 1572872 | tf_op jit(solution)/shard_map/ppermute | solution.py:128
  86.0 19.4 %collective-permute-start.13 = (bf16[256,2048]{1,0:T(8,128)(2,1)}, bf16[256,2048]{1,0:T(8,128)(2,1)S(1)}, u32[]{:S(2)}, u32[]{:S(2)}) collective-permute-start(bf16[256,2048]{1,0:T(8,128)(2,1)} %collective-permute-done.12.refs_0_), channel_id=1, source_target_pairs={{0,1},{1,0},{2,3},{3,2},{4,5},{5,4},{6,7},{7,6},{8,9},{9,8},{10,11... | collective-permute-start | bytes 3145736 | tf_op jit(solution)/shard_map/ppermute | solution.py:137
  87.4 16.8 %collective-permute-start.33 = (bf16[384,768]{1,0:T(8,128)(2,1)S(1)}, bf16[384,768]{1,0:T(8,128)(2,1)S(1)}, u32[]{:S(2)}, u32[]{:S(2)}) collective-permute-start(bf16[384,768]{1,0:T(8,128)(2,1)S(1)} %collective-permute-done.10.refs_5_), channel_id=1, source_target_pairs={{0,8},{2,10},{4,12},{6,14},{8,24},{10,26},{12,28},{14,30},{16,0},{... | collective-permute-start | bytes 1769480 | tf_op jit(solution)/shard_map/ppermute | solution.py:131
  96.7 20.7 %collective-permute-start.25 = (bf16[512,768]{1,0:T(8,128)(2,1)S(1)}, bf16[512,768]{1,0:T(8,128)(2,1)S(1)}, u32[]{:S(2)}, u32[]{:S(2)}) collective-permute-start(bf16[512,768]{1,0:T(8,128)(2,1)S(1)} %copy-done.8), channel_id=1, source_target_pairs={{0,6},{2,4},{4,2},{6,0},{8,14},{10,12},{12,10},{14,8},{16,22},{18,... | collective-permute-start | bytes 2359304 | tf_op jit(solution)/shard_map/ppermute | solution.py:128
  97.3 12.3 %collective-permute-start.23 = (bf16[128,2048]{1,0:T(8,128)(2,1)S(1)}, bf16[128,2048]{1,0:T(8,128)(2,1)S(1)}, u32[]{:S(2)}, u32[]{:S(2)}) collective-permute-start(bf16[128,2048]{1,0:T(8,128)(2,1)S(1)} %collective-permute-done.21.refs_0_), channel_id=1, source_target_pairs={{0,1},{1,0},{2,3},{3,2},{4,5},{5,4},{6,7},{7,6},{8,9},{9,8},{10,11... | collective-permute-start | bytes 1572872 | tf_op jit(solution)/shard_map/ppermute | solution.py:137
  105.9 28.3 %collective-permute-start.19 = (bf16[512,768]{1,0:T(8,128)(2,1)S(1)}, bf16[512,768]{1,0:T(8,128)(2,1)S(1)}, u32[]{:S(2)}, u32[]{:S(2)}) collective-permute-start(bf16[512,768]{1,0:T(8,128)(2,1)S(1)} %copy-done.7), channel_id=1, source_target_pairs={{0,4},{2,6},{4,0},{6,2},{8,12},{10,14},{12,8},{14,10},{16,20},{18,... | collective-permute-start | bytes 2359304 | tf_op jit(solution)/shard_map/ppermute | solution.py:128
  109.6 33.0 %collective-permute-start.11 = (bf16[256,1536]{1,0:T(8,128)(2,1)S(1)}, bf16[256,1536]{1,0:T(8,128)(2,1)S(1)}, u32[]{:S(2)}, u32[]{:S(2)}) collective-permute-start(bf16[256,1536]{1,0:T(8,128)(2,1)S(1)} %slice.177), channel_id=1, source_target_pairs={{0,1},{1,0},{2,3},{3,2},{4,5},{5,4},{6,7},{7,6},{8,9},{9,8},{10,11... | collective-permute-start | bytes 2359304 | tf_op jit(solution)/shard_map/ppermute | solution.py:137
  110.0 33.4 %collective-permute-start.34 = (bf16[256,512]{1,0:T(8,128)(2,1)S(1)}, bf16[256,512]{1,0:T(8,128)(2,1)S(1)}, u32[]{:S(2)}, u32[]{:S(2)}) collective-permute-start(bf16[256,512]{1,0:T(8,128)(2,1)S(1)} %slice.201), channel_id=1, source_target_pairs={{0,1},{1,0},{2,3},{3,2},{4,5},{5,4},{6,7},{7,6},{8,9},{9,8},{10,11... | collective-permute-start | bytes 786440 | tf_op jit(solution)/shard_map/ppermute | solution.py:137
  144.2 23.9 %collective-permute-start.42 = (bf16[256,256]{1,0:T(8,128)(2,1)S(1)}, bf16[256,256]{1,0:T(8,128)(2,1)S(1)}, u32[]{:S(2)}, u32[]{:S(2)}) collective-permute-start(bf16[256,256]{1,0:T(8,128)(2,1)S(1)} %get-tuple-element.45), channel_id=1, source_target_pairs={{0,4},{2,6},{4,0},{6,2},{8,12},{10,14},{12,8},{14,10},{16,20},{18,... | collective-permute-start | bytes 393224 | tf_op jit(solution)/shard_map/ppermute | solution.py:128
  144.9 24.4 %collective-permute-start.39 = (bf16[256,256]{1,0:T(8,128)(2,1)S(1)}, bf16[256,256]{1,0:T(8,128)(2,1)S(1)}, u32[]{:S(2)}, u32[]{:S(2)}) collective-permute-start(bf16[256,256]{1,0:T(8,128)(2,1)S(1)} %get-tuple-element.44), channel_id=1, source_target_pairs={{0,2},{2,0},{4,6},{6,4},{8,10},{10,8},{12,14},{14,12},{16,18},{18,... | collective-permute-start | bytes 393224 | tf_op jit(solution)/shard_map/ppermute | solution.py:128
  147.8 21.7 %collective-permute-start.16 = (bf16[256,768]{1,0:T(8,128)(2,1)S(1)}, bf16[256,768]{1,0:T(8,128)(2,1)S(1)}, u32[]{:S(2)}, u32[]{:S(2)}) collective-permute-start(bf16[256,768]{1,0:T(8,128)(2,1)S(1)} %slice.305), channel_id=1, source_target_pairs={{0,2},{2,0},{4,6},{6,4},{8,10},{10,8},{12,14},{14,12},{16,18},{18,... | collective-permute-start | bytes 1179656 | tf_op jit(solution)/shard_map/ppermute | solution.py:128
  149.3 17.8 %collective-permute-start.27 = (bf16[256,768]{1,0:T(8,128)(2,1)S(1)}, bf16[256,768]{1,0:T(8,128)(2,1)S(1)}, u32[]{:S(2)}, u32[]{:S(2)}) collective-permute-start(bf16[256,768]{1,0:T(8,128)(2,1)S(1)} %get-tuple-element.40), channel_id=1, source_target_pairs={{0,2},{2,0},{4,6},{6,4},{8,10},{10,8},{12,14},{14,12},{16,18},{18,... | collective-permute-start | bytes 1179656 | tf_op jit(solution)/shard_map/ppermute | solution.py:128
  158.2 12.5 %collective-permute-start.29 = (bf16[256,768]{1,0:T(8,128)(2,1)S(1)}, bf16[256,768]{1,0:T(8,128)(2,1)S(1)}, u32[]{:S(2)}, u32[]{:S(2)}) collective-permute-start(bf16[256,768]{1,0:T(8,128)(2,1)S(1)} %slice.304), channel_id=1, source_target_pairs={{0,4},{2,6},{4,0},{6,2},{8,12},{10,14},{12,8},{14,10},{16,20},{18,... | collective-permute-start | bytes 1179656 | tf_op jit(solution)/shard_map/ppermute | solution.py:128
  169.3 26.4 %collective-permute-start.45 = (bf16[384,512]{1,0:T(8,128)(2,1)S(1)}, bf16[384,512]{1,0:T(8,128)(2,1)S(1)}, u32[]{:S(2)}, u32[]{:S(2)}) collective-permute-start(bf16[384,512]{1,0:T(8,128)(2,1)S(1)} %get-tuple-element.24), channel_id=1, source_target_pairs={{0,8},{2,10},{4,12},{6,14},{8,16},{10,18},{12,20},{14,22},{16,24},... | collective-permute-start | bytes 1179656 | tf_op jit(solution)/shard_map/ppermute | solution.py:134
  169.5 32.5 %collective-permute-start.46 = (bf16[384,512]{1,0:T(8,128)(2,1)S(1)}, bf16[384,512]{1,0:T(8,128)(2,1)S(1)}, u32[]{:S(2)}, u32[]{:S(2)}) collective-permute-start(bf16[384,512]{1,0:T(8,128)(2,1)S(1)} %get-tuple-element.26), channel_id=1, source_target_pairs={{0,16},{2,18},{4,20},{6,22},{8,24},{10,26},{12,28},{14,30},{16,0},... | collective-permute-start | bytes 1179656 | tf_op jit(solution)/shard_map/ppermute | solution.py:134
  170.6 32.7 %collective-permute-start.47 = (bf16[384,512]{1,0:T(8,128)(2,1)S(1)}, bf16[384,512]{1,0:T(8,128)(2,1)S(1)}, u32[]{:S(2)}, u32[]{:S(2)}) collective-permute-start(bf16[384,512]{1,0:T(8,128)(2,1)S(1)} %get-tuple-element.25), channel_id=1, source_target_pairs={{0,24},{2,26},{4,28},{6,30},{8,0},{10,2},{12,4},{14,6},{16,8},{18,... | collective-permute-start | bytes 1179656 | tf_op jit(solution)/shard_map/ppermute | solution.py:134
  187.1 27.4 %collective-permute-start.32 = (bf16[256,1536]{1,0:T(8,128)(2,1)S(1)}, bf16[256,1536]{1,0:T(8,128)(2,1)S(1)}, u32[]{:S(2)}, u32[]{:S(2)}) collective-permute-start(bf16[256,1536]{1,0:T(8,128)(2,1)S(1)} %pad_maximum_fusion.7.refs_0_), channel_id=1, source_target_pairs={{0,1},{1,0},{2,3},{3,2},{4,5},{5,4},{6,7},{7,6},{8,9},{9,8},{10,11... | collective-permute-start | bytes 2359304 | tf_op jit(solution)/shard_map/ppermute | solution.py:137
  187.7 26.8 %collective-permute-start.44 = (bf16[256,512]{1,0:T(8,128)(2,1)S(1)}, bf16[256,512]{1,0:T(8,128)(2,1)S(1)}, u32[]{:S(2)}, u32[]{:S(2)}) collective-permute-start(bf16[256,512]{1,0:T(8,128)(2,1)S(1)} %pad_maximum_fusion.16.refs_2_), channel_id=1, source_target_pairs={{0,1},{1,0},{2,3},{3,2},{4,5},{5,4},{6,7},{7,6},{8,9},{9,8},{10,11... | collective-permute-start | bytes 786440 | tf_op jit(solution)/shard_map/ppermute | solution.py:137
  (30 other events, 297.9 us)
